TPU v7x, 256 devices: a whole 4x4x8 slice. The times are simulated.
256 devices in a mesh: rep: 32 (over z, y), fs: 4 (over x), tp: 2 (over core).
Axes of the slice: x: 4, y: 4, z: 8, core: 2. Of those that a mesh axis runs over, the one named last changes fastest.
Arguments:
- tokens: bfloat16 [32768, 2048], P(('rep', 'fs', 'tp')), may hold values from -24 to 24
- cotangent: bfloat16 [32768, 2048], P(('rep', 'fs', 'tp')), may hold values from -24 to 24
- gate_weight: bfloat16 [2048, 3072], P(None, 'fs'), may hold values from -0.125 to 0.125
- up_weight: bfloat16 [2048, 3072], P(None, 'fs'), may hold values from -0.125 to 0.125
- down_weight_t: bfloat16 [2048, 3072], P(None, 'fs'), may hold values from -0.109375 to 0.109375
Outputs:
- input_grad: bfloat16 [32768, 2048], P(('rep', 'fs', 'tp'))
- gate_grad: float32 [2048, 3072], P(('rep', 'tp'), 'fs')
- up_grad: float32 [2048, 3072], P(('rep', 'tp'), 'fs')
- down_grad: float32 [2048, 3072], P(('rep', 'tp'), 'fs')
All inputs are finite; a program needn't handle non-finite values.
Results may differ from a plain program's by a relative error of at most 0.012.
Values may be sent and summed in bfloat16 or wider, within the bound.
A program may use at most 128 MiB of HBM per device.

v0:
```python
import jax
import jax.numpy as jnp
from jax import lax
from jax.sharding import PartitionSpec as P


def joined_along(parts, dim):
    parts = jnp.moveaxis(parts, 0, dim)
    shape = parts.shape
    return parts.reshape(*shape[:dim], shape[dim] * shape[dim + 1], *shape[dim + 2 :])


def copy_for_each(value, axis):
    copies = jnp.broadcast_to(value, (lax.axis_size(axis), *value.shape))
    return lax.all_to_all(copies, axis, split_axis=0, concat_axis=0, tiled=True)


def gathered_copies(value, axis, dim):
    return joined_along(copy_for_each(value, axis), dim)


def in_one_piece(arrays, axis, dim, along):
    widths = [a.shape[along] for a in arrays]
    both = jnp.concatenate(arrays, axis=along)
    whole = gathered_copies(both, axis, dim)
    return tuple(jnp.split(whole, [sum(widths[:k]) for k in range(1, len(widths))], axis=along))


def in_blocks(value, dim, peers):
    before, after = (value.shape[:dim], value.shape[dim + 1 :])
    return jnp.moveaxis(value.reshape(*before, peers, -1, *after), dim, 0)


def sum_at_owner(value, axis, dim):
    parts = in_blocks(value, dim, lax.axis_size(axis))
    arrived = lax.all_to_all(parts, axis, split_axis=0, concat_axis=0, tiled=True)
    return arrived.astype(jnp.float32).sum(axis=0)


def in_one_piece_2(arrays, axis, dim, along):
    both = jnp.concatenate(arrays, axis=along)
    whole, at, finished = (lax.psum_scatter(both, axis, scatter_dimension=dim, tiled=True), 0, [])
    for a in arrays:
        finished.append(lax.slice_in_dim(whole, at, at + a.shape[along], axis=along))
        at += a.shape[along]
    return tuple(finished)


def on_device(tokens, cotangent, gate_weight, up_weight, down_weight_t):
    tok_rows, cot_rows = in_one_piece((tokens, cotangent), "fs", 0, 1)
    gate_pre = jnp.dot(tok_rows, gate_weight, preferred_element_type=jnp.float32)
    up_pre = jnp.dot(tok_rows, up_weight, preferred_element_type=jnp.float32)
    sig_gate = jax.nn.sigmoid(gate_pre)
    act_gate = gate_pre * sig_gate
    hidden = (act_gate * up_pre).astype(jnp.bfloat16)
    hid_grad = jnp.dot(cot_rows, down_weight_t, preferred_element_type=jnp.float32)
    local_gate_back = (hid_grad * up_pre * sig_gate * (1.0 + gate_pre * (1.0 - sig_gate))).astype(
        jnp.bfloat16
    )
    local_up_back = (hid_grad * act_gate).astype(jnp.bfloat16)
    tok_all, cot_all, gate_back, up_back, hidden = (
        tok_rows,
        cot_rows,
        local_gate_back,
        local_up_back,
        hidden,
    )
    own_rows = tokens.shape[0]
    across = (((1,), (1,)), ((), ()))
    input_grad = sum_at_owner(
        (
            lax.dot_general(gate_back, gate_weight, across, preferred_element_type=jnp.float32)
            + lax.dot_general(up_back, up_weight, across, preferred_element_type=jnp.float32)
        ).astype(jnp.bfloat16),
        "fs",
        0,
    ).astype(jnp.bfloat16)
    replicas = lax.axis_size("rep")
    cores = lax.axis_size("tp")
    shards = lax.axis_size("fs")
    grad_scale = float(own_rows * replicas * shards * cores) ** (-0.5)
    down_rows = (((0,), (0,)), ((), ()))
    gate_local = (
        lax.dot_general(tok_all, gate_back, down_rows, preferred_element_type=jnp.float32)
        * grad_scale
    )
    up_local = (
        lax.dot_general(tok_all, up_back, down_rows, preferred_element_type=jnp.float32)
        * grad_scale
    )
    down_local = (
        lax.dot_general(cot_all, hidden, down_rows, preferred_element_type=jnp.float32) * grad_scale
    )
    summed = in_one_piece_2((gate_local, up_local, down_local), ("rep", "tp"), 0, 1)
    return (input_grad, summed[0], summed[1], summed[2])


def solution(mesh):
    return jax.shard_map(
        on_device,
        mesh=mesh,
        in_specs=(
            P(("rep", "fs", "tp"), None),
            P(("rep", "fs", "tp"), None),
            P(None, "fs"),
            P(None, "fs"),
            P(None, "fs"),
        ),
        out_specs=(
            P(("rep", "fs", "tp"), None),
            P(("rep", "tp"), "fs"),
            P(("rep", "tp"), "fs"),
            P(("rep", "tp"), "fs"),
        ),
        check_vma=False,
    )
```

profile of v0, /device:TPU:1, one launch (start us, length us, event | category | flops | bytes accessed | tf_op | source)
XLA Modules:
  0.0 303.5 jit_solution(6540316080608797469)
XLA Ops:
  7.2 0.0 copy-start
  7.2 0.0 reduce-scatter.4.cloned.1.call-start
  7.2 1.4 pad_maximum_fusion.1
  8.7 0.5 broadcast_in_dim.3
  9.2 52.4 %all_to_all.10 = bf16[4,128,4096]{2,1,0:T(8,128)(2,1)S(1)} all-to-all(bf16[4,128,4096]{2,1,0:T(8,128)(2,1)S(1)} %broadcast_in_dim.3), channel_id=1, replica_groups=mesh['rep'=32,'fs'=4,'tp'=2] {'fs'}, dimensions={0} | all-to-all | bytes 8388608 | tf_op jit(solution)/shard_map/all_to_all | solution.py:15
  61.6 0.0 copy-done
  61.6 0.0 copy-start.5
  61.6 1.8 fusion.6
  63.4 0.1 copy-done.5
  63.5 1.8 fusion.8
  65.3 0.0 copy-start.4
  65.3 2.0 convolution_multiply_fusion
  67.3 0.0 copy-done.4
  67.3 2.2 multiply_convert_fusion.1
  69.5 0.0 copy-start.1
  69.5 0.0 copy-start.3
  69.5 1.9 convolution_multiply_fusion.1
  71.4 0.0 copy-done.1
  71.4 0.0 copy-done.3
  71.4 1.9 convolution_multiply_fusion.2
  73.3 7.1 %pad_maximum_fusion = f32[2048,2304]{0,1:T(8,128)} fusion(f32[2048,768]{0,1:T(8,128)S(1)} %convolution_multiply_fusion, f32[2048,768]{0,1:T(8,128)S(1)} %convolution_multiply_fusion.1, f32[2048,768]{0,1:T(8,128)S(1)} %convolution_multiply_fusion.2), kind=kLoop, calls=%fused_computation | loop fusion | flops 9437184 | bytes 37748736 | tf_op jit(solution)/shard_map/concatenate | solution.py:41
  80.4 18.7 %copy.15 = f32[2048,2304]{1,0:T(8,128)} copy(f32[2048,2304]{0,1:T(8,128)} %pad_maximum_fusion) | data formatting | bytes 37748736
  99.1 0.0 reduce-scatter.4.cloned.1.call-update
  99.2 0.0 copy-start.2
  99.2 0.0 copy-start.6
  99.2 3.1 %fusion.13 = f32[512,2048]{1,0:T(8,128)S(1)} fusion(bf16[512,768]{1,0:T(8,128)(2,1)} %copy-done.3, bf16[2048,768]{1,0:T(8,128)(2,1)S(1)} %copy-done), kind=kOutput, calls=%fused_computation.22 | convolution fusion | flops 1610612736 | bytes 8126464 | tf_op jit(solution)/shard_map/dot_general | solution.py:72
  102.3 0.0 copy-done.2
  102.3 0.0 copy-done.6
  102.3 1.8 add_convert_fusion
  104.1 27.7 %all_to_all.11 = bf16[4,128,2048]{2,1,0:T(8,128)(2,1)} all-to-all(bf16[4,128,2048]{2,1,0:T(8,128)(2,1)S(1)} %bitcast.18), channel_id=1, replica_groups=mesh['rep'=32,'fs'=4,'tp'=2] {'fs'}, dimensions={0} | all-to-all | bytes 4194304 | tf_op jit(solution)/shard_map/all_to_all | solution.py:36
  131.8 3.0 reduce_sum.12
  134.8 160.1 %reduce-scatter.4.cloned.1.call-done = f32[32,2304]{1,0:T(8,128)} async-done(((f32[2048,2304]{1,0:T(8,128)}), f32[32,2304]{1,0:T(8,128)}) %reduce-scatter.4.cloned.1.call-update) | async-done | bytes 294928
  295.0 1.7 fusion.12
Async XLA Ops:
  7.2 54.4 %copy-start = (bf16[2048,768]{1,0:T(8,128)(2,1)S(1)}, bf16[2048,768]{1,0:T(8,128)(2,1)}, u32[]{:S(2)}) copy-start(bf16[2048,768]{1,0:T(8,128)(2,1)} %param.7) | copy-start | bytes 9437188
  7.2 287.8 %reduce-scatter.4.cloned.1.call-start = ((), (), s32[]{:S(2)}) async-start(), calls=%async_computation.3 | async-start | bytes 19169280
  61.6 1.9 copy-start.5
  65.3 2.0 copy-start.4
  69.5 1.9 copy-start.1
  69.5 1.9 copy-start.3
  99.2 3.1 %copy-start.2 = (bf16[512,768]{1,0:T(8,128)(2,1)S(1)}, bf16[512,768]{1,0:T(8,128)(2,1)}, u32[]{:S(2)}) copy-start(bf16[512,768]{1,0:T(8,128)(2,1)} %copy-done.1) | copy-start | bytes 2359300
  99.2 3.1 %copy-start.6 = (bf16[2048,768]{1,0:T(8,128)(2,1)S(1)}, bf16[2048,768]{1,0:T(8,128)(2,1)}, u32[]{:S(2)}) copy-start(bf16[2048,768]{1,0:T(8,128)(2,1)} %param.8) | copy-start | bytes 9437188
Sparse Core Ops, SparseCore 0:
  99.3 195.6 reduce-scatter.3
where the time goes:
time: 307 us; the launch traced here: 304 us
  waiting for transfers between devices  160 us (52%)
  blocking collectives  80.1 us (26%)
  local copies, waits for them, and re-layouts  21 us (7%)
  matrix products  16.5 us (5%)
  between operations  14.2 us (5%)
  other arithmetic  11.6 us (4%)
    unnamed x2, waiting for transfers between devices  160 us
    all_to_all x1, blocking collectives, copy_for_each(): return lax.all_to_all(copies, axis, split_axis=0, concat_axis=0, tiled=True)  52.4 us
    all_to_all x1, blocking collectives, sum_at_owner(): lax.all_to_all(parts, axis, split_axis=0, concat_axis=0, tiled=True)  27.7 us
    unnamed x15, local copies, waits for them, and re-layouts  18.8 us
    concatenate x1, other arithmetic, in_one_piece_2(): both = jnp.concatenate(arrays, axis=along)  7.1 us
  transfers between devices with their start and end apart: 1, of which 1 were waited for; matrix products, arithmetic and copies ran while one was open for 3% of the time, Pallas kernels for 0%

commit v1 on v0

--- a/solution.py
+++ b/solution.py
@@ -22,7 +22,7 @@
 def in_one_piece(arrays, axis, dim, along):
     widths = [a.shape[along] for a in arrays]
     both = jnp.concatenate(arrays, axis=along)
-    whole = gathered_copies(both, axis, dim)
+    whole = lax.all_gather(both, axis, axis=dim, tiled=True)
     return tuple(jnp.split(whole, [sum(widths[:k]) for k in range(1, len(widths))], axis=along))
 
 
@@ -38,10 +38,12 @@
 
 
 def in_one_piece_2(arrays, axis, dim, along):
-    both = jnp.concatenate(arrays, axis=along)
+    both = jnp.concatenate([a.astype(jnp.bfloat16) for a in arrays], axis=along)
     whole, at, finished = (lax.psum_scatter(both, axis, scatter_dimension=dim, tiled=True), 0, [])
     for a in arrays:
-        finished.append(lax.slice_in_dim(whole, at, at + a.shape[along], axis=along))
+        finished.append(
+            lax.slice_in_dim(whole, at, at + a.shape[along], axis=along).astype(jnp.float32)
+        )
         at += a.shape[along]
     return tuple(finished)
 

time: 307 us -> 262 us (0.85)
  blocking collectives: 80.1 us -> 28.6 us
  waiting for transfers between devices: 160 us -> 169 us
  local copies, waits for them, and re-layouts: 21 us -> 16.8 us
    all_gather x0 -> x1, waiting for transfers between devices: none -> 54.5 us  [in_one_piece(): whole = lax.all_gather(both, axis, axis=dim, tiled=True)]
    all_to_all x1 -> x0, blocking collectives: 52.4 us -> none  [copy_for_each(): return lax.all_to_all(copies, axis, split_axis=0, concat_axis=0, tiled=True)]
    unnamed x2 -> x3, waiting for transfers between devices: 160 us -> 115 us
    unnamed x15 -> x23, local copies, waits for them, and re-layouts: 18.8 us -> 15.9 us
  transfers between devices with their start and end apart: 1 -> 2, of which waited for: 1 -> 2; matrix products, arithmetic and copies ran while one was open for 3% -> 3% of each run, Pallas kernels for 0% -> 0%
where the time goes in v1:
time: 262 us; the launch traced here: 257 us
  waiting for transfers between devices  169 us (65%)
  blocking collectives  28.6 us (11%)
  matrix products  18 us (7%)
  local copies, waits for them, and re-layouts  16.8 us (6%)
  between operations  14.2 us (5%)
  other arithmetic  10.1 us (4%)
    unnamed x3, waiting for transfers between devices  115 us
    all_gather x1, waiting for transfers between devices, in_one_piece(): whole = lax.all_gather(both, axis, axis=dim, tiled=True)  54.5 us
    all_to_all x1, blocking collectives, sum_at_owner(): lax.all_to_all(parts, axis, split_axis=0, concat_axis=0, tiled=True)  28.6 us
    unnamed x23, local copies, waits for them, and re-layouts  15.9 us
  transfers between devices with their start and end apart: 2, of which 2 were waited for; matrix products, arithmetic and copies ran while one was open for 3% of the time, Pallas kernels for 0%

profile of v1, /device:TPU:1, one launch (start us, length us, event | category | flops | bytes accessed | tf_op | source)
XLA Modules:
  0.0 257.0 jit_solution(10101316856633388367)
XLA Ops:
  7.2 0.0 copy-start
  7.2 0.0 all-gather.2.cloned.1.call-start
  7.2 2.4 pad_maximum_fusion.1
  9.6 0.0 all-gather.2.cloned.1.call-update
  9.7 0.0 reduce-scatter.4.cloned.1.call-start
  9.7 54.5 %all-gather.2.cloned.1.call-done = bf16[512,4096]{1,0:T(8,128)(2,1)} async-done(((bf16[128,4096]{1,0:T(8,128)(2,1)}), bf16[512,4096]{1,0:T(8,128)(2,1)}) %all-gather.2.cloned.1.call-update) | async-done | bytes 4194320 | tf_op jit(solution)/shard_map/all_gather | solution.py:25
  64.2 0.0 copy-done
  64.2 0.0 copy-start.1
  64.2 0.0 copy-start.3
  64.2 3.5 %fusion.6 = f32[512,768]{1,0:T(8,128)S(1)} fusion(bf16[2048,768]{1,0:T(8,128)(2,1)S(1)} %copy-done, bf16[512,4096]{1,0:T(8,128)(2,1)} %all-gather.2.cloned.1.call-done), kind=kOutput, calls=%fused_computation.15 | convolution fusion | flops 1610612736 | bytes 6815744 | tf_op jit(solution)/shard_map/dot_general | solution.py:53
  67.7 0.0 copy-done.1
  67.7 0.3 copy-done.3
  68.0 1.8 fusion.8
  69.8 0.0 copy-start.2
  69.8 1.9 multiply_convert_fusion
  71.7 0.0 copy-done.2
  71.8 2.1 multiply_convert_fusion.4
  73.9 0.0 copy-start.5
  73.9 0.0 copy-start.7
  73.9 1.8 multiply_convert_fusion.1
  75.8 0.0 copy-done.5
  75.8 0.0 copy-done.7
  75.8 1.8 multiply_convert_fusion.2
  77.6 4.7 %pad_maximum_fusion = bf16[2048,2304]{0,1:T(8,128)(2,1)} fusion(bf16[2048,768]{0,1:T(8,128)(2,1)S(1)} %multiply_convert_fusion, bf16[2048,768]{0,1:T(8,128)(2,1)S(1)} %multiply_convert_fusion.1, bf16[2048,768]{0,1:T(8,128)(2,1)S(1)} %multiply_convert_fusion.2), kind=kLoop, calls=%fused_computation | loop fusion | flops 28311552 | bytes 18874368 | tf_op jit(solution)/shard_map/concatenate | solution.py:41
  82.3 12.8 %copy.15 = bf16[2048,2304]{1,0:T(8,128)(2,1)} copy(bf16[2048,2304]{0,1:T(8,128)(2,1)} %pad_maximum_fusion) | data formatting | bytes 18874368
  95.1 0.0 reduce-scatter.4.cloned.1.call-update
  95.1 0.0 copy-start.4
  95.2 0.0 copy-start.6
  95.2 3.1 %fusion.13 = f32[512,2048]{1,0:T(8,128)S(1)} fusion(bf16[512,768]{1,0:T(8,128)(2,1)} %copy-done.7, bf16[2048,768]{1,0:T(8,128)(2,1)S(1)} %copy-done), kind=kOutput, calls=%fused_computation.22 | convolution fusion | flops 1610612736 | bytes 8126464 | tf_op jit(solution)/shard_map/dot_general | solution.py:74
  98.3 0.0 copy-done.4
  98.3 0.0 copy-done.6
  98.3 1.8 add_convert_fusion
  100.1 28.6 %all_to_all.5 = bf16[4,128,2048]{2,1,0:T(8,128)(2,1)} all-to-all(bf16[4,128,2048]{2,1,0:T(8,128)(2,1)S(1)} %bitcast.11), channel_id=1, replica_groups=mesh['rep'=32,'fs'=4,'tp'=2] {'fs'}, dimensions={0} | all-to-all | bytes 4194304 | tf_op jit(solution)/shard_map/all_to_all | solution.py:36
  128.8 3.0 %reduce_sum.12 = bf16[128,2048]{1,0:T(8,128)(2,1)} reduce(bf16[4,128,2048]{2,1,0:T(8,128)(2,1)} %all_to_all.5, bf16[]{:T(256)} %constant.2.clone.1), dimensions={0}, to_apply=%region_0.0 | reduce | flops 786432 | bytes 2621442 | tf_op jit(solution)/shard_map/reduce_sum | solution.py:37
  131.7 114.8 %reduce-scatter.4.cloned.1.call-done = bf16[32,2304]{1,0:T(8,128)(2,1)} async-done(((bf16[2048,2304]{1,0:T(8,128)(2,1)}), bf16[32,2304]{1,0:T(8,128)(2,1)}) %reduce-scatter.4.cloned.1.call-update) | async-done | bytes 147472
  246.5 0.9 fusion.12
  247.4 0.2 copy.17
  247.6 0.8 copy.12
  248.3 0.2 copy.18
  248.5 0.8 copy.13
  249.3 0.2 copy.19
  249.4 0.8 copy.14
Async XLA Ops:
  7.2 57.0 %copy-start = (bf16[2048,768]{1,0:T(8,128)(2,1)S(1)}, bf16[2048,768]{1,0:T(8,128)(2,1)}, u32[]{:S(2)}) copy-start(bf16[2048,768]{1,0:T(8,128)(2,1)} %param.7) | copy-start | bytes 9437188
  7.2 57.0 %all-gather.2.cloned.1.call-start = ((), (), s32[]{:S(2)}) async-start(), calls=%async_computation.2 | async-start | bytes 5242880 | tf_op jit(solution)/shard_map/all_gather | solution.py:25
  9.7 236.9 %reduce-scatter.4.cloned.1.call-start = ((), (), s32[]{:S(2)}) async-start(), calls=%async_computation.3 | async-start | bytes 9584640
  64.2 3.5 %copy-start.1 = (bf16[512,4096]{1,0:T(8,128)(2,1)S(1)}, bf16[512,4096]{1,0:T(8,128)(2,1)}, u32[]{:S(2)}) copy-start(bf16[512,4096]{1,0:T(8,128)(2,1)} %all-gather.2.cloned.1.call-done) | copy-start | bytes 12582916
  64.2 3.8 %copy-start.3 = (bf16[2048,768]{1,0:T(8,128)(2,1)S(1)}, bf16[2048,768]{1,0:T(8,128)(2,1)}, u32[]{:S(2)}) copy-start(bf16[2048,768]{1,0:T(8,128)(2,1)} %param.8) | copy-start | bytes 9437188
  69.8 1.9 copy-start.2
  73.9 1.9 copy-start.5
  73.9 1.9 copy-start.7
  95.1 3.1 %copy-start.4 = (bf16[2048,768]{1,0:T(8,128)(2,1)S(1)}, bf16[2048,768]{1,0:T(8,128)(2,1)}, u32[]{:S(2)}) copy-start(bf16[2048,768]{1,0:T(8,128)(2,1)} %param.8) | copy-start | bytes 9437188
  95.2 3.1 %copy-start.6 = (bf16[512,768]{1,0:T(8,128)(2,1)S(1)}, bf16[512,768]{1,0:T(8,128)(2,1)}, u32[]{:S(2)}) copy-start(bf16[512,768]{1,0:T(8,128)(2,1)} %copy-done.5) | copy-start | bytes 2359300
Sparse Core Ops, SparseCore 0:
  9.8 54.3 all-gather.1
  95.3 151.2 reduce-scatter.3

commit v2 on v0

v2 whole, which is shorter than its diff:
```python
import functools
import heapq

import jax
import jax.numpy as jnp
from jax import lax
from jax.experimental import pallas as pl
from jax.experimental.pallas import tpu as pltpu
from jax.sharding import PartitionSpec as P

MESH = pl.DeviceIdType.MESH
F32 = jnp.float32
BF16 = jnp.bfloat16

NY, NZ = 4, 8
BLOCKS = ((0, 256, "z"), (256, 256, "y"), (512, 256, "z"), (768, 256, "y"), (1024, 128, "z"))


def chains_of(n):
    return ((1, 0, n // 2), (-1, 1, n // 2), (1, 1, n // 2 - 1), (-1, 0, n // 2 - 1))


class Ring:
    def __init__(self, block, phase, axis, first_slot):
        self.block, self.phase, self.axis = block, phase, axis
        self.n = NY if axis == "y" else NZ
        self.chains = chains_of(self.n)
        self.slots, at = {}, 0
        for c, (_, _, start) in enumerate(self.chains):
            for d in range(start, 0, -1):
                self.slots[c, d] = at
                at += 1
        self.count, self.first_slot = at, first_slot

    def half_shape(self):
        width = BLOCKS[self.block][1]
        if self.phase == 2:
            return (32, width)
        return (NZ // 2, 64, width) if self.axis == "y" else (NY // 2, 64, width)

    def half_bytes(self):
        size = 2
        for extent in self.half_shape():
            size *= extent
        return size


def all_rings():
    rings, slot = {}, 0
    for b, (_, _, first) in enumerate(BLOCKS):
        for phase, axis in ((1, first), (2, "z" if first == "y" else "y")):
            rings[b, phase] = Ring(b, phase, axis, slot)
            slot += rings[b, phase].count
    return rings, slot


def schedule(rings, rate=46.0e3, latency=2.7, step=0.2):
    free, arrivals, order, left, tick = {}, [], [], {}, [0]

    def send(key, c, d, now):
        ring = rings[key]
        link = (ring.axis, ring.chains[c][0])
        free[link] = max(free.get(link, 0.0), now) + ring.half_bytes() / rate
        tick[0] += 1
        heapq.heappush(arrivals, (free[link] + latency, tick[0], key, c, d))

    def begin(key, now):
        left[key] = 4
        for c, (_, _, start) in enumerate(rings[key].chains):
            send(key, c, start, now)

    for b in range(len(BLOCKS)):
        begin((b, 1), 0.0)
    now = 0.0
    while arrivals:
        at, _, key, c, d = heapq.heappop(arrivals)
        now = max(now, at) + step
        order.append((key, c, d))
        if d > 1:
            send(key, c, d - 1, now)
        else:
            left[key] -= 1
            if left[key] == 0 and key[1] == 1:
                begin((key[0], 2), now)
    return order, now


def kernel(tok_hbm, cot_hbm, wg_hbm, wu_hbm, wd_hbm,
           ig_out, gate_out, up_out, down_out,
           xb, wgu, wd, gub, hid, acc, own_ig, ig_part, ig_send0, ig_send, ig_recv0, ig_recv,
           xr1, xr2, *rest):
    nb = len(BLOCKS)
    blks, rest = rest[:nb], rest[nb:]
    rings, total_slots = all_rings()
    keys = [(b, phase) for b in range(nb) for phase in (1, 2)]
    rbufs, rest = dict(zip(keys, rest[: 2 * nb])), rest[2 * nb :]
    fins, rest = rest[:nb], rest[nb:]
    finr, rest = rest[:nb], rest[nb:]
    (load_sem, ag_send, ag_recv, rel_send, rel_recv, igx_send, igx_recv,
     xrs_send, xrs_recv, ring_send, ring_recv, fin_send, fin_recv) = rest

    rep, x, core = lax.axis_index("rep"), lax.axis_index("fs"), lax.axis_index("tp")
    z, y = rep // NY, lax.rem(rep, NY)
    right = (rep, lax.rem(x + 1, 4), core)
    left = (rep, lax.rem(x + 3, 4), core)
    partner = (rep, x, 1 - core)
    y_of = {s: (z * NY + lax.rem(y + s + NY, NY), x, core) for s in (1, -1)}
    z_of = {s: (lax.rem(z + s + NZ, NZ) * NY + y, x, core) for s in (1, -1)}

    def remote(src, dst, send_sem, recv_sem, to):
        return pltpu.make_async_remote_copy(src_ref=src, dst_ref=dst, send_sem=send_sem,
                                            recv_sem=recv_sem, device_id=to, device_id_type=MESH)

    cols = pl.ds(pl.multiple_of(core * 384, 128), 384)
    load_tok = pltpu.make_async_copy(tok_hbm, xb.at[0, 0], load_sem.at[0])
    load_cot = pltpu.make_async_copy(cot_hbm, xb.at[0, 1], load_sem.at[1])
    load_w = [
        pltpu.make_async_copy(wg_hbm.at[:, cols], wgu.at[:, pl.ds(0, 384)], load_sem.at[2]),
        pltpu.make_async_copy(wu_hbm.at[:, cols], wgu.at[:, pl.ds(384, 384)], load_sem.at[3]),
        pltpu.make_async_copy(wd_hbm.at[:, cols], wd, load_sem.at[4]),
    ]
    load_tok.start()
    load_cot.start()
    for copy in load_w:
        copy.start()

    barrier = pltpu.get_barrier_semaphore()
    for other in (right, left, partner, y_of[1], y_of[-1], z_of[1], z_of[-1]):
        pl.semaphore_signal(barrier, inc=1, device_id=other, device_id_type=MESH)
    pl.semaphore_wait(barrier, 7)
    load_tok.wait()
    load_cot.wait()

    def own_piece(k, side):
        piece = k if side == 0 else (k + 2) % 4
        return remote(xb.at[0, :, pl.ds(32 * piece, 32)], xb.at[2 + k, :, pl.ds(32 * side, 32)],
                      ag_send.at[side, k], ag_recv.at[side, k], right if side == 0 else left)

    def passed_on(k, side):
        return remote(xb.at[2 + k, :, pl.ds(32 * side, 32)], xb.at[6 + k, :, pl.ds(32 * side, 32)],
                      ag_send.at[side, 4 + k], ag_recv.at[side, 4 + k], right if side == 0 else left)

    def arrival(k, side):
        here = xb.at[2 + k, :, pl.ds(32 * side, 32)]
        return remote(here, here, ag_send.at[side, k], ag_recv.at[side, k],
                      right if side == 0 else left)

    def relay(k):
        return remote(xb.at[2 + k, :, pl.ds(0, 64)], xb.at[2 + k, :, pl.ds(64, 64)],
                      rel_send.at[k], rel_recv.at[k], partner)

    own_to_partner = remote(xb.at[0], xb.at[1], rel_send.at[6], rel_recv.at[6], partner)
    for k in range(4):
        for side in (0, 1):
            own_piece(k, side).start()
        if k == 0:
            own_to_partner.start()
    for copy in load_w:
        copy.wait()

    def forward(s):
        rows = pl.ds(pl.multiple_of(s * 128, 128), 128)
        gu = jnp.dot(xb[s, 0], wgu[...], preferred_element_type=F32)
        hg = jnp.dot(xb[s, 1], wd[...], preferred_element_type=F32)
        gate, up = gu[:, :384], gu[:, 384:]
        sig = jax.nn.sigmoid(gate)
        act = gate * sig
        gub[rows, pl.ds(0, 384)] = (hg * up * sig * (1.0 + gate * (1.0 - sig))).astype(BF16)
        gub[rows, pl.ds(384, 384)] = (hg * act).astype(BF16)
        hid[rows, :] = (act * up).astype(BF16)

    def input_part(s, store):
        rows = pl.ds(pl.multiple_of(s * 128, 128), 128)

        def some(n, carry):
            d = pl.ds(pl.multiple_of(n * 512, 512), 512)
            part = lax.dot_general(gub[rows, :], wgu[d, :], (((1,), (1,)), ((), ())),
                                   preferred_element_type=F32)
            store(d, part.astype(BF16))
            return carry

        lax.fori_loop(0, 4, some, 0)

    def store_own(d, part):
        own_ig[:, d] = part

    def store_partner(d, part):
        ig_send0[:, d] = part

    send_ig0 = remote(ig_send0, ig_recv0, igx_send.at[6], igx_recv.at[6], partner)

    def send_ig(k):
        return remote(ig_send.at[k], ig_recv.at[k], igx_send.at[k], igx_recv.at[k], partner)

    def step_part(s):
        k = s - 2

        def store(d, part):
            ig_part[k, :, d] = part[:64]
            ig_send[k, :, d] = part[64:]

        input_part(s, store)
        send_ig(k).start()

    forward(0)
    input_part(0, store_own)
    own_to_partner.wait_recv()
    forward(1)
    input_part(1, store_partner)
    send_ig0.start()

    def take(k):
        arrival(k, 0).wait_recv()
        arrival(k, 1).wait_recv()
        relay(k).start()

    def early(k, carry):
        take(k)

        @pl.when(k < 2)
        def _():
            passed_on(k, 0).start()
            passed_on(k, 1).start()

        relay(k).wait_recv()
        forward(k + 2)
        step_part(k + 2)
        return carry

    lax.fori_loop(0, 4, early, 0)

    across = (((0,), (0,)), ((), ()))

    def products(j, first, count):
        d = pl.ds(pl.multiple_of(j * 256, 256), 256)
        rows = pl.ds(first * 128, count * 128)
        tok = xb[pl.ds(first, count), 0, :, d].reshape(count * 128, 256)
        cot = xb[pl.ds(first, count), 1, :, d].reshape(count * 128, 256)
        return (lax.dot_general(tok, gub[rows, :], across, preferred_element_type=F32),
                lax.dot_general(cot, hid[rows, :], across, preferred_element_type=F32))

    def first_sums(j, carry):
        a, b = products(j, 0, 6)
        acc[j, :, pl.ds(0, 768)] = a
        acc[j, :, pl.ds(768, 384)] = b
        return carry

    lax.fori_loop(0, 8, first_sums, 0)

    take(4)
    relay(4).wait_recv()
    forward(6)
    step_part(6)
    take(5)
    relay(5).wait_recv()
    forward(7)

    def last_sums(j, carry):
        a, b = products(j, 6, 2)
        a = (acc[j, :, pl.ds(0, 768)] + a).astype(BF16)
        b = (acc[j, :, pl.ds(768, 384)] + b).astype(BF16)
        for i, (col, width, _) in enumerate(BLOCKS):
            piece = a[:, col : col + width] if col < 768 else b[:, col - 768 : col - 768 + width]
            blks[i][j] = piece.reshape(NY, 64, width)
        return carry

    lax.fori_loop(0, 8, last_sums, 0)

    def half_of(ring, j, half):
        blk = blks[ring.block]
        if ring.phase == 1:
            if ring.axis == "y":
                return blk.at[pl.ds(4 * half, 4), j]
            return blk.at[j, pl.ds(2 * half, 2)]
        if ring.axis == "z":
            return blk.at[j, y, pl.ds(32 * half, 32)]
        return blk.at[z, j, pl.ds(32 * half, 32)]

    def place(ring, offset):
        if ring.axis == "y":
            return lax.rem(y + offset + NY, NY)
        return lax.rem(z + offset + NZ, NZ)

    def hop(key, c, d):
        ring = rings[key]
        sign, half, _ = ring.chains[c]
        slot = ring.slots[c, d]
        sem = ring.first_slot + slot
        return remote(half_of(ring, place(ring, sign * d), half), rbufs[key].at[slot],
                      ring_send.at[sem], ring_recv.at[sem],
                      (y_of if ring.axis == "y" else z_of)[sign])

    def begin(key):
        for c, (_, _, start) in enumerate(rings[key].chains):
            hop(key, c, start).start()

    def add_into(dst, src):
        shape = dst.shape
        if len(shape) == 2:
            dst[...] = (dst[...].astype(F32) + src[...].astype(F32)).astype(BF16)
        else:
            def one(i, carry):
                dst[i] = (dst[i].astype(F32) + src[i].astype(F32)).astype(BF16)
                return carry
            lax.fori_loop(0, shape[0], one, 0)

    for b in range(nb):
        begin((b, 1))

    step_part(7)

    def xrs(stage, way):
        rows = pl.ds(32 * way, 32)
        which = {0: (4, 2), 1: (2, 2), 2: (0, 2)}[stage]
        dst = xr1.at[way] if stage == 0 else xr2.at[way, pl.ds(which[0], 2)]
        return remote(ig_part.at[pl.ds(which[0], 2), rows], dst, xrs_send.at[stage, way],
                      xrs_recv.at[stage, way], left if way == 0 else right)

    def merge_part(k, carry):
        send_ig(k).wait_recv()
        ig_part[k] = (ig_part[k].astype(F32) + ig_recv[k].astype(F32)).astype(BF16)
        return carry

    lax.fori_loop(2, 6, merge_part, 0)
    for stage in (0, 1):
        for way in (0, 1):
            xrs(stage, way).start()
    lax.fori_loop(0, 2, merge_part, 0)
    send_ig0.wait_recv()

    def x_middle():
        for way in (0, 1):
            xrs(0, way).wait_recv()
        for k in range(2):
            for way in (0, 1):
                rows = pl.ds(32 * way, 32)
                ig_part[k, rows, :] = (ig_part[k, rows, :].astype(F32)
                                       + xr1[way, k].astype(F32)).astype(BF16)
        for way in (0, 1):
            xrs(2, way).start()

    def x_end():
        for stage in (1, 2):
            for way in (0, 1):
                xrs(stage, way).wait_recv()
        for piece in range(4):
            rows = pl.ds(32 * piece, 32)
            total = own_ig[rows, :].astype(F32) + ig_recv0[rows, :].astype(F32)
            total = total + xr2[0, piece].astype(F32) + xr2[1, (piece + 2) % 4].astype(F32)
            ig_out[rows, :] = total.astype(BF16)

    order, _ = schedule(rings)
    left_of = {key: 4 for key in keys}
    scale = float(32768) ** -0.5

    def fin_copy(b):
        return remote(fins[b].at[pl.ds(pl.multiple_of((1 - core) * 32, 32), 32)], finr[b],
                      fin_send.at[b], fin_recv.at[b], partner)

    def finish_block(b):
        ring = rings[b, 2]
        for half in (0, 1):
            total = half_of(rings[b, 2], place(ring, 0), half)[...].astype(F32)
            for c, (_, h, _) in enumerate(ring.chains):
                if h == half:
                    total = total + rbufs[b, 2][ring.slots[c, 1]].astype(F32)
            fins[b][pl.ds(32 * half, 32), :] = total * scale
        fin_copy(b).start()

    for at, (key, c, d) in enumerate(order):
        ring = rings[key]
        sign, half, _ = ring.chains[c]
        hop(key, c, d).wait_recv()
        if d > 1:
            add_into(half_of(ring, place(ring, sign * (d - 1)), half), rbufs[key].at[ring.slots[c, d]])
            hop(key, c, d - 1).start()
        else:
            left_of[key] -= 1
            if key[1] == 1:
                add_into(half_of(ring, place(ring, 0), half), rbufs[key].at[ring.slots[c, d]])
                if left_of[key] == 0:
                    begin((key[0], 2))
            elif left_of[key] == 0:
                finish_block(key[0])
        if at == 3 * len(order) // 10:
            x_middle()
        if at == 7 * len(order) // 10:
            x_end()

    def place_out(b, value, which):
        col, width, _ = BLOCKS[b]
        at = col
        while at < col + width:
            take_n = min(384 - at % 384, col + width - at)
            out = (gate_out, up_out, down_out)[at // 384]
            out[:, pl.ds(pl.multiple_of(which * 384 + at % 384, 128), take_n)] = (
                value[:, at - col : at - col + take_n])
            at += take_n

    mine = pl.ds(pl.multiple_of(core * 32, 32), 32)
    for b in range(nb):
        place_out(b, fins[b][mine, :], core)
    for b in range(nb):
        fin_copy(b).wait_recv()
        place_out(b, finr[b][...], 1 - core)

    for k in range(4):
        for side in (0, 1):
            own_piece(k, side).wait_send()
    for k in range(2):
        for side in (0, 1):
            passed_on(k, side).wait_send()
    for k in range(6):
        relay(k).wait_send()
        send_ig(k).wait_send()
    own_to_partner.wait_send()
    send_ig0.wait_send()
    for stage in range(3):
        for way in (0, 1):
            xrs(stage, way).wait_send()
    for key, c, d in order:
        hop(key, c, d).wait_send()
    for b in range(nb):
        fin_copy(b).wait_send()


def on_device(tokens, cotangent, gate_weight, up_weight, down_weight_t):
    rings, slots = all_rings()
    keys = [(b, phase) for b in range(len(BLOCKS)) for phase in (1, 2)]
    anywhere = pl.BlockSpec(memory_space=pl.ANY)
    vmem = pl.BlockSpec(memory_space=pltpu.VMEM)
    dma = pltpu.SemaphoreType.DMA
    return pl.pallas_call(
        kernel,
        out_shape=(
            jax.ShapeDtypeStruct((128, 2048), BF16),
            jax.ShapeDtypeStruct((32, 768), F32),
            jax.ShapeDtypeStruct((32, 768), F32),
            jax.ShapeDtypeStruct((32, 768), F32),
        ),
        in_specs=[anywhere] * 5,
        out_specs=[vmem] * 4,
        scratch_shapes=[
            pltpu.VMEM((8, 2, 128, 2048), BF16),
            pltpu.VMEM((2048, 768), BF16),
            pltpu.VMEM((2048, 384), BF16),
            pltpu.VMEM((1024, 768), BF16),
            pltpu.VMEM((1024, 384), BF16),
            pltpu.VMEM((8, 256, 1152), F32),
            pltpu.VMEM((128, 2048), BF16),
            pltpu.VMEM((6, 64, 2048), BF16),
            pltpu.VMEM((128, 2048), BF16),
            pltpu.VMEM((6, 64, 2048), BF16),
            pltpu.VMEM((128, 2048), BF16),
            pltpu.VMEM((6, 64, 2048), BF16),
            pltpu.VMEM((2, 2, 32, 2048), BF16),
            pltpu.VMEM((2, 4, 32, 2048), BF16),
        ]
        + [pltpu.VMEM((NZ, NY, 64, width), BF16) for _, width, _ in BLOCKS]
        + [pltpu.VMEM((rings[key].count, *rings[key].half_shape()), BF16) for key in keys]
        + [pltpu.VMEM((64, width), F32) for _, width, _ in BLOCKS]
        + [pltpu.VMEM((32, width), F32) for _, width, _ in BLOCKS]
        + [
            dma((5,)), dma((2, 6)), dma((2, 6)), dma((7,)), dma((7,)), dma((7,)), dma((7,)),
            dma((3, 2)), dma((3, 2)), dma((slots,)), dma((slots,)),
            dma((len(BLOCKS),)), dma((len(BLOCKS),)),
        ],
        compiler_params=pltpu.CompilerParams(
            collective_id=0, has_side_effects=True, vmem_limit_bytes=62 * 1024 * 1024
        ),
    )(tokens, cotangent, gate_weight, up_weight, down_weight_t)


def solution(mesh):
    rows, tall = P(("rep", "fs", "tp"), None), P(("rep", "tp"), "fs")
    return jax.shard_map(
        on_device,
        mesh=mesh,
        in_specs=(rows, rows, P(None, "fs"), P(None, "fs"), P(None, "fs")),
        out_specs=(rows, tall, tall, tall),
        check_vma=False,
    )
```

time: 307 us -> 102 us (0.33); the launches traced: 304 us -> 102 us
  waiting for transfers between devices: 160 us -> 0 us
  Pallas kernels: 0 us -> 94.7 us
  blocking collectives: 80.1 us -> 0 us
  matrix products: 16.5 us -> 0 us
  local copies, waits for them, and re-layouts: 21 us -> 6.5 us
  between operations: 14.2 us -> 0.64 us
  other arithmetic: 11.6 us -> 0 us
    unnamed x2 -> x0, waiting for transfers between devices: 160 us -> none
    pallas_call x0 -> x1, Pallas kernels: none -> 94.7 us  [on_device(): pl.pallas_call(kernel, out_shape=(jax.ShapeDtypeStruct((128, 2048), BF16)...]
    all_to_all x2 -> x0, blocking collectives: 80.1 us -> none  [the longest x1 52.4 us: copy_for_each(): return lax.all_to_all(copies, axis, split_axis=0, concat_axis=0, tiled=True)]
    dot_general x8 -> x0, matrix products: 16.5 us -> none  [the longest x1 3.11 us: on_device(): lax.dot_general(gate_back, gate_weight, across, preferred_element_type=jn...]
    unnamed x15 -> x4, local copies, waits for them, and re-layouts: 18.8 us -> 6.5 us
    concatenate x2 -> x0, other arithmetic: 8.54 us -> none  [the longest x1 7.1 us: in_one_piece_2(): both = jnp.concatenate(arrays, axis=along)]
  transfers between devices with their start and end apart: 1 -> 0, of which waited for: 1 -> 0; matrix products, arithmetic and copies ran while one was open for 3% -> 0% of each run, Pallas kernels for 0% -> 0%
where the time goes in v2:
time: 102 us
  Pallas kernels  94.7 us (93%)
  local copies, waits for them, and re-layouts  6.5 us (6%)
    pallas_call x1, Pallas kernels, on_device(): pl.pallas_call(kernel, out_shape=(jax.ShapeDtypeStruct((128, 2048), BF16)...  94.7 us
    unnamed x4, local copies, waits for them, and re-layouts  6.5 us

profile of v2, /device:TPU:1, one launch (start us, length us, event | category | flops | bytes accessed | tf_op | source)
XLA Modules:
  0.0 101.9 jit_solution(16261596888904328761)
XLA Ops:
  0.6 94.7 %shard_map.84 = (bf16[128,2048]{1,0:T(8,128)(2,1)}, f32[32,768]{1,0:T(8,128)}, f32[32,768]{1,0:T(8,128)}, f32[32,768]{1,0:T(8,128)}) custom-call(bf16[128,2048]{1,0:T(8,128)(2,1)} %tok_hbm.1, bf16[128,2048]{1,0:T(8,128)(2,1)} %cot_hbm.1, bf16[2048,768]{1,0:T(8,128)(2,1)} %wg_hbm.1, bf16[2048,768]{1,0:T(8,128)(2,1)} %wu_hbm.1, bf16[2048,768]{1,0:T(8,128)(2,1)} %wd_hbm.1), custom_call_target="tpu_custom_call" | custom-call | tf_op jit(solution)/shard_map/pallas_call | solution.py:433
  95.4 1.9 %copy.13 = bf16[128,2048]{1,0:T(8,128)(2,1)} copy(bf16[128,2048]{1,0:T(8,128)(2,1)} %get-tuple-element.8) | data formatting | bytes 1048576
  97.2 1.5 %copy.14 = f32[32,768]{1,0:T(8,128)} copy(f32[32,768]{1,0:T(8,128)} %get-tuple-element.9) | data formatting | bytes 196608
  98.8 1.5 %copy.15 = f32[32,768]{1,0:T(8,128)} copy(f32[32,768]{1,0:T(8,128)} %get-tuple-element.10) | data formatting | bytes 196608
  100.3 1.5 %copy.16 = f32[32,768]{1,0:T(8,128)} copy(f32[32,768]{1,0:T(8,128)} %get-tuple-element.11) | data formatting | bytes 196608

commit v3 on v2

--- a/solution.py
+++ b/solution.py
@@ -11,24 +11,38 @@
 MESH = pl.DeviceIdType.MESH
 F32 = jnp.float32
 BF16 = jnp.bfloat16
+VMEM_LIMIT = 56 * 1024 * 1024
 
 NY, NZ = 4, 8
-BLOCKS = ((0, 256, "z"), (256, 256, "y"), (512, 256, "z"), (768, 256, "y"), (1024, 128, "z"))
-
-
-def chains_of(n):
-    return ((1, 0, n // 2), (-1, 1, n // 2), (1, 1, n // 2 - 1), (-1, 0, n // 2 - 1))
+X_BEGIN, X_MIDDLE, X_END = 6.0, 14.0, 26.0
+BLOCKS = ((0, 256, "z", "r"), (256, 256, "z", "r"), (512, 128, "y", "t"), (640, 128, "y", "t"), (768, 128, "y", "t"), (896, 256, "y", "t"))
+
+
+Y_RING = ((1, 0, ((2, 1), (1, 1))), (-1, 1, ((2, 1), (1, 1))), (1, 1, ((1, 1),)), (-1, 0, ((1, 1),)))
+Z_RING = (
+    (1, 0, ((4, 1), (3, 1), (2, 1), (1, 1))), (-1, 1, ((4, 1), (3, 1), (2, 1), (1, 1))),
+    (1, 1, ((3, 1), (2, 1), (1, 1))), (-1, 0, ((3, 1), (2, 1), (1, 1))),
+)
+Z_TWO = (
+    (1, 0, ((4, 2), (2, 2))), (-1, 1, ((4, 2), (2, 2))),
+    (1, 0, ((3, 2), (1, 1))), (1, 1, ((3, 2), (1, 1))),
+    (-1, 0, ((3, 2), (1, 1))), (-1, 1, ((3, 2), (1, 1))),
+    (1, 1, ((2, 2),)), (-1, 0, ((2, 2),)),
+)
+CHAINS = {("y", "r"): Y_RING, ("z", "r"): Z_RING, ("z", "t"): Z_TWO}
+OFFSETS = (4, 3, -3, 2, -2, 1, -1, 0)
+SLAB = {offset: r for r, offset in enumerate(OFFSETS)}
+SLAB[-4] = 0
 
 
 class Ring:
-    def __init__(self, block, phase, axis, first_slot):
+    def __init__(self, block, phase, axis, style, first_slot):
         self.block, self.phase, self.axis = block, phase, axis
-        self.n = NY if axis == "y" else NZ
-        self.chains = chains_of(self.n)
+        self.chains = CHAINS[axis, style]
         self.slots, at = {}, 0
-        for c, (_, _, start) in enumerate(self.chains):
-            for d in range(start, 0, -1):
-                self.slots[c, d] = at
+        for c, (_, _, hops) in enumerate(self.chains):
+            for i in range(len(hops)):
+                self.slots[c, i] = at
                 at += 1
         self.count, self.first_slot = at, first_slot
 
@@ -44,44 +58,64 @@
             size *= extent
         return size
 
+    def last(self, c):
+        return self.slots[c, len(self.chains[c][2]) - 1]
+
+    def ready(self, c):
+        _, half, hops = self.chains[c]
+        if self.axis == "y":
+            return 3 if half == 0 else 7
+        return SLAB[self.chains[c][0] * hops[0][0]]
+
 
 def all_rings():
     rings, slot = {}, 0
-    for b, (_, _, first) in enumerate(BLOCKS):
+    for b, (_, _, first, style) in enumerate(BLOCKS):
         for phase, axis in ((1, first), (2, "z" if first == "y" else "y")):
-            rings[b, phase] = Ring(b, phase, axis, slot)
+            rings[b, phase] = Ring(b, phase, axis, "r" if phase == 1 else style, slot)
             slot += rings[b, phase].count
     return rings, slot
 
 
-def schedule(rings, rate=46.0e3, latency=2.7, step=0.2):
+def first_sends(rings):
+    groups = [[] for _ in OFFSETS]
+    for b in range(len(BLOCKS)):
+        ring = rings[b, 1]
+        for c in range(len(ring.chains)):
+            groups[ring.ready(c)].append((b, c))
+    return groups
+
+
+def schedule(rings, rate=46.0e3, latency=3.0, hop=0.75, step=0.06, slab=0.36):
     free, arrivals, order, left, tick = {}, [], [], {}, [0]
 
-    def send(key, c, d, now):
+    def send(key, c, i, now):
         ring = rings[key]
-        link = (ring.axis, ring.chains[c][0])
-        free[link] = max(free.get(link, 0.0), now) + ring.half_bytes() / rate
+        sign, _, hops = ring.chains[c]
+        link = (ring.axis, sign)
+        wire = ring.half_bytes() / rate
+        start = max(free.get(link, 0.0), now)
+        free[link] = start + wire * hops[i][1]
         tick[0] += 1
-        heapq.heappush(arrivals, (free[link] + latency, tick[0], key, c, d))
-
-    def begin(key, now):
-        left[key] = 4
-        for c, (_, _, start) in enumerate(rings[key].chains):
-            send(key, c, start, now)
-
-    for b in range(len(BLOCKS)):
-        begin((b, 1), 0.0)
+        heapq.heappush(arrivals, (start + wire + latency + hop * (hops[i][1] - 1), tick[0], key, c, i))
+
+    for key in rings:
+        left[key] = len(rings[key].chains)
+    for r, group in enumerate(first_sends(rings)):
+        for b, c in group:
+            send((b, 1), c, 0, slab * (r + 1))
     now = 0.0
     while arrivals:
-        at, _, key, c, d = heapq.heappop(arrivals)
+        at, _, key, c, i = heapq.heappop(arrivals)
         now = max(now, at) + step
-        order.append((key, c, d))
-        if d > 1:
-            send(key, c, d - 1, now)
+        order.append((now, key, c, i))
+        if i + 1 < len(rings[key].chains[c][2]):
+            send(key, c, i + 1, now)
         else:
             left[key] -= 1
             if left[key] == 0 and key[1] == 1:
-                begin((key[0], 2), now)
+                for k in range(len(rings[key[0], 2].chains)):
+                    send((key[0], 2), k, 0, now)
     return order, now
 
 
@@ -104,8 +138,10 @@
     right = (rep, lax.rem(x + 1, 4), core)
     left = (rep, lax.rem(x + 3, 4), core)
     partner = (rep, x, 1 - core)
+    far = any(ring.chains is Z_TWO for ring in rings.values())
     y_of = {s: (z * NY + lax.rem(y + s + NY, NY), x, core) for s in (1, -1)}
-    z_of = {s: (lax.rem(z + s + NZ, NZ) * NY + y, x, core) for s in (1, -1)}
+    z_of = {s: (lax.rem(z + s + NZ, NZ) * NY + y, x, core)
+            for s in ((1, -1, 2, -2) if far else (1, -1))}
 
     def remote(src, dst, send_sem, recv_sem, to):
         return pltpu.make_async_remote_copy(src_ref=src, dst_ref=dst, send_sem=send_sem,
@@ -125,9 +161,10 @@
         copy.start()
 
     barrier = pltpu.get_barrier_semaphore()
-    for other in (right, left, partner, y_of[1], y_of[-1], z_of[1], z_of[-1]):
+    others = (right, left, partner, *y_of.values(), *z_of.values())
+    for other in others:
         pl.semaphore_signal(barrier, inc=1, device_id=other, device_id_type=MESH)
-    pl.semaphore_wait(barrier, 7)
+    pl.semaphore_wait(barrier, len(others))
     load_tok.wait()
     load_cot.wait()
 
@@ -245,54 +282,35 @@
         acc[j, :, pl.ds(768, 384)] = b
         return carry
 
-    lax.fori_loop(0, 8, first_sums, 0)
-
+    lax.fori_loop(0, 4, first_sums, 0)
     take(4)
+    lax.fori_loop(4, 8, first_sums, 0)
     relay(4).wait_recv()
     forward(6)
+    take(5)
     step_part(6)
-    take(5)
     relay(5).wait_recv()
     forward(7)
 
-    def last_sums(j, carry):
-        a, b = products(j, 6, 2)
-        a = (acc[j, :, pl.ds(0, 768)] + a).astype(BF16)
-        b = (acc[j, :, pl.ds(768, 384)] + b).astype(BF16)
-        for i, (col, width, _) in enumerate(BLOCKS):
-            piece = a[:, col : col + width] if col < 768 else b[:, col - 768 : col - 768 + width]
-            blks[i][j] = piece.reshape(NY, 64, width)
-        return carry
-
-    lax.fori_loop(0, 8, last_sums, 0)
-
-    def half_of(ring, j, half):
+    def half_of(ring, offset, half):
         blk = blks[ring.block]
+        if ring.axis == "y":
+            there = lax.rem(y + offset + NY, NY)
+            if ring.phase == 1:
+                return blk.at[pl.ds(4 * half, 4), there]
+            return blk.at[SLAB[0], there, pl.ds(32 * half, 32)]
         if ring.phase == 1:
-            if ring.axis == "y":
-                return blk.at[pl.ds(4 * half, 4), j]
-            return blk.at[j, pl.ds(2 * half, 2)]
-        if ring.axis == "z":
-            return blk.at[j, y, pl.ds(32 * half, 32)]
-        return blk.at[z, j, pl.ds(32 * half, 32)]
-
-    def place(ring, offset):
-        if ring.axis == "y":
-            return lax.rem(y + offset + NY, NY)
-        return lax.rem(z + offset + NZ, NZ)
-
-    def hop(key, c, d):
+            return blk.at[SLAB[offset], pl.ds(2 * half, 2)]
+        return blk.at[SLAB[offset], y, pl.ds(32 * half, 32)]
+
+    def hop(key, c, i):
         ring = rings[key]
-        sign, half, _ = ring.chains[c]
-        slot = ring.slots[c, d]
+        sign, half, hops = ring.chains[c]
+        slot = ring.slots[c, i]
         sem = ring.first_slot + slot
-        return remote(half_of(ring, place(ring, sign * d), half), rbufs[key].at[slot],
+        return remote(half_of(ring, sign * hops[i][0], half), rbufs[key].at[slot],
                       ring_send.at[sem], ring_recv.at[sem],
-                      (y_of if ring.axis == "y" else z_of)[sign])
-
-    def begin(key):
-        for c, (_, _, start) in enumerate(rings[key].chains):
-            hop(key, c, start).start()
+                      (y_of if ring.axis == "y" else z_of)[sign * hops[i][1]])
 
     def add_into(dst, src):
         shape = dst.shape
@@ -304,8 +322,16 @@
                 return carry
             lax.fori_loop(0, shape[0], one, 0)
 
-    for b in range(nb):
-        begin((b, 1))
+    for r, group in enumerate(first_sends(rings)):
+        j = lax.rem(z + OFFSETS[r] + NZ, NZ)
+        a, b = products(j, 6, 2)
+        a = (acc[j, :, pl.ds(0, 768)] + a).astype(BF16)
+        b = (acc[j, :, pl.ds(768, 384)] + b).astype(BF16)
+        for i, (col, width, _, _) in enumerate(BLOCKS):
+            piece = a[:, col : col + width] if col < 768 else b[:, col - 768 : col - 768 + width]
+            blks[i][r] = piece.reshape(NY, 64, width)
+        for block, c in group:
+            hop((block, 1), c, 0).start()
 
     step_part(7)
 
@@ -321,12 +347,13 @@
         ig_part[k] = (ig_part[k].astype(F32) + ig_recv[k].astype(F32)).astype(BF16)
         return carry
 
-    lax.fori_loop(2, 6, merge_part, 0)
-    for stage in (0, 1):
-        for way in (0, 1):
-            xrs(stage, way).start()
-    lax.fori_loop(0, 2, merge_part, 0)
-    send_ig0.wait_recv()
+    def x_begin():
+        lax.fori_loop(2, 6, merge_part, 0)
+        for stage in (0, 1):
+            for way in (0, 1):
+                xrs(stage, way).start()
+        lax.fori_loop(0, 2, merge_part, 0)
+        send_ig0.wait_recv()
 
     def x_middle():
         for way in (0, 1):
@@ -350,7 +377,7 @@
             ig_out[rows, :] = total.astype(BF16)
 
     order, _ = schedule(rings)
-    left_of = {key: 4 for key in keys}
+    left_of = {key: len(rings[key].chains) for key in keys}
     scale = float(32768) ** -0.5
 
     def fin_copy(b):
@@ -360,35 +387,38 @@
     def finish_block(b):
         ring = rings[b, 2]
         for half in (0, 1):
-            total = half_of(rings[b, 2], place(ring, 0), half)[...].astype(F32)
+            total = half_of(ring, 0, half)[...].astype(F32)
             for c, (_, h, _) in enumerate(ring.chains):
                 if h == half:
-                    total = total + rbufs[b, 2][ring.slots[c, 1]].astype(F32)
+                    total = total + rbufs[b, 2][ring.last(c)].astype(F32)
             fins[b][pl.ds(32 * half, 32), :] = total * scale
         fin_copy(b).start()
 
-    for at, (key, c, d) in enumerate(order):
+    todo = [(X_BEGIN, x_begin), (X_MIDDLE, x_middle), (X_END, x_end)]
+    for at, key, c, i in order:
+        while todo and at > todo[0][0]:
+            todo.pop(0)[1]()
         ring = rings[key]
-        sign, half, _ = ring.chains[c]
-        hop(key, c, d).wait_recv()
-        if d > 1:
-            add_into(half_of(ring, place(ring, sign * (d - 1)), half), rbufs[key].at[ring.slots[c, d]])
-            hop(key, c, d - 1).start()
+        sign, half, hops = ring.chains[c]
+        hop(key, c, i).wait_recv()
+        if i + 1 < len(hops):
+            add_into(half_of(ring, sign * hops[i + 1][0], half), rbufs[key].at[ring.slots[c, i]])
+            hop(key, c, i + 1).start()
         else:
             left_of[key] -= 1
             if key[1] == 1:
-                add_into(half_of(ring, place(ring, 0), half), rbufs[key].at[ring.slots[c, d]])
+                add_into(half_of(ring, 0, half), rbufs[key].at[ring.slots[c, i]])
                 if left_of[key] == 0:
-                    begin((key[0], 2))
+                    second = (key[0], 2)
+                    for k in range(len(rings[second].chains)):
+                        hop(second, k, 0).start()
             elif left_of[key] == 0:
                 finish_block(key[0])
-        if at == 3 * len(order) // 10:
-            x_middle()
-        if at == 7 * len(order) // 10:
-            x_end()
+    for _, act in todo:
+        act()
 
     def place_out(b, value, which):
-        col, width, _ = BLOCKS[b]
+        col, width, _, _ = BLOCKS[b]
         at = col
         while at < col + width:
             take_n = min(384 - at % 384, col + width - at)
@@ -418,10 +448,19 @@
     for stage in range(3):
         for way in (0, 1):
             xrs(stage, way).wait_send()
-    for key, c, d in order:
-        hop(key, c, d).wait_send()
+    for _, key, c, i in order:
+        hop(key, c, i).wait_send()
     for b in range(nb):
         fin_copy(b).wait_send()
+
+
+def write_out(a, b, c, d, out_a, out_b, out_c, out_d, sems):
+    copies = [pltpu.make_async_copy(src, dst, sems.at[i])
+              for i, (src, dst) in enumerate(((a, out_a), (b, out_b), (c, out_c), (d, out_d)))]
+    for copy in copies:
+        copy.start()
+    for copy in copies:
+        copy.wait()
 
 
 def on_device(tokens, cotangent, gate_weight, up_weight, down_weight_t):
@@ -430,7 +469,7 @@
     anywhere = pl.BlockSpec(memory_space=pl.ANY)
     vmem = pl.BlockSpec(memory_space=pltpu.VMEM)
     dma = pltpu.SemaphoreType.DMA
-    return pl.pallas_call(
+    results = pl.pallas_call(
         kernel,
         out_shape=(
             jax.ShapeDtypeStruct((128, 2048), BF16),
@@ -456,19 +495,27 @@
             pltpu.VMEM((2, 2, 32, 2048), BF16),
             pltpu.VMEM((2, 4, 32, 2048), BF16),
         ]
-        + [pltpu.VMEM((NZ, NY, 64, width), BF16) for _, width, _ in BLOCKS]
+        + [pltpu.VMEM((NZ, NY, 64, width), BF16) for _, width, _, _ in BLOCKS]
         + [pltpu.VMEM((rings[key].count, *rings[key].half_shape()), BF16) for key in keys]
-        + [pltpu.VMEM((64, width), F32) for _, width, _ in BLOCKS]
-        + [pltpu.VMEM((32, width), F32) for _, width, _ in BLOCKS]
+        + [pltpu.VMEM((64, width), F32) for _, width, _, _ in BLOCKS]
+        + [pltpu.VMEM((32, width), F32) for _, width, _, _ in BLOCKS]
         + [
             dma((5,)), dma((2, 6)), dma((2, 6)), dma((7,)), dma((7,)), dma((7,)), dma((7,)),
             dma((3, 2)), dma((3, 2)), dma((slots,)), dma((slots,)),
             dma((len(BLOCKS),)), dma((len(BLOCKS),)),
         ],
         compiler_params=pltpu.CompilerParams(
-            collective_id=0, has_side_effects=True, vmem_limit_bytes=62 * 1024 * 1024
+            collective_id=0, has_side_effects=True, vmem_limit_bytes=VMEM_LIMIT
         ),
     )(tokens, cotangent, gate_weight, up_weight, down_weight_t)
+    return pl.pallas_call(
+        write_out,
+        out_shape=tuple(jax.ShapeDtypeStruct(r.shape, r.dtype) for r in results),
+        in_specs=[vmem] * 4,
+        out_specs=[anywhere] * 4,
+        scratch_shapes=[dma((4,))],
+        compiler_params=pltpu.CompilerParams(vmem_limit_bytes=4 * 1024 * 1024),
+    )(*results)
 
 
 def solution(mesh):

time: 102 us -> 93.8 us (0.920)
  Pallas kernels: 94.7 us -> 89.2 us
  local copies, waits for them, and re-layouts: 6.5 us -> 3.71 us
    pallas_call x1, Pallas kernels: 94.7 us -> 88.3 us  [on_device(): pl.pallas_call(kernel, out_shape=(jax.ShapeDtypeStruct((128, 2048), BF16)...]
    unnamed x4 -> x8, local copies, waits for them, and re-layouts: 6.5 us -> 3.71 us
where the time goes in v3:
time: 93.8 us; the launch traced here: 93.6 us
  Pallas kernels  89.2 us (95%)
  local copies, waits for them, and re-layouts  3.71 us (4%)
    pallas_call x1, Pallas kernels, on_device(): pl.pallas_call(kernel, out_shape=(jax.ShapeDtypeStruct((128, 2048), BF16)...  88.3 us
    unnamed x8, local copies, waits for them, and re-layouts  3.71 us

profile of v3, /device:TPU:1, one launch (start us, length us, event | category | flops | bytes accessed | tf_op | source)
XLA Modules:
  0.0 93.6 jit_solution(15773596863032358485)
XLA Ops:
  0.6 88.3 %shard_map.84 = (bf16[128,2048]{1,0:T(8,128)(2,1)}, f32[32,768]{1,0:T(8,128)}, f32[32,768]{1,0:T(8,128)}, f32[32,768]{1,0:T(8,128)}) custom-call(bf16[128,2048]{1,0:T(8,128)(2,1)} %tok_hbm.1, bf16[128,2048]{1,0:T(8,128)(2,1)} %cot_hbm.1, bf16[2048,768]{1,0:T(8,128)(2,1)} %wg_hbm.1, bf16[2048,768]{1,0:T(8,128)(2,1)} %wu_hbm.1, bf16[2048,768]{1,0:T(8,128)(2,1)} %wd_hbm.1), custom_call_target="tpu_custom_call" | custom-call | tf_op jit(solution)/shard_map/pallas_call | solution.py:472
  89.0 0.0 copy-start
  89.0 1.0 %copy-done = bf16[128,2048]{1,0:T(8,128)(2,1)S(1)} copy-done((bf16[128,2048]{1,0:T(8,128)(2,1)S(1)}, bf16[128,2048]{1,0:T(8,128)(2,1)}, u32[]{:S(2)}) %copy-start) | copy-done | bytes 524312
  90.0 0.0 copy-start.1
  90.0 0.9 copy-done.1
  90.9 0.0 copy-start.2
  90.9 0.9 copy-done.2
  91.8 0.0 copy-start.3
  91.8 0.9 copy-done.3
  92.7 0.9 shard_map.85
Async XLA Ops:
  89.0 1.0 %copy-start = (bf16[128,2048]{1,0:T(8,128)(2,1)S(1)}, bf16[128,2048]{1,0:T(8,128)(2,1)}, u32[]{:S(2)}) copy-start(bf16[128,2048]{1,0:T(8,128)(2,1)} %get-tuple-element.8.a) | copy-start | bytes 1572868
  90.0 0.9 copy-start.1
  90.9 0.9 copy-start.2
  91.8 0.9 copy-start.3

commit v4 on v3

--- a/solution.py
+++ b/solution.py
@@ -472,10 +472,10 @@
     results = pl.pallas_call(
         kernel,
         out_shape=(
-            jax.ShapeDtypeStruct((128, 2048), BF16),
-            jax.ShapeDtypeStruct((32, 768), F32),
-            jax.ShapeDtypeStruct((32, 768), F32),
-            jax.ShapeDtypeStruct((32, 768), F32),
+            pltpu.VMEM((128, 2048), BF16),
+            pltpu.VMEM((32, 768), F32),
+            pltpu.VMEM((32, 768), F32),
+            pltpu.VMEM((32, 768), F32),
         ),
         in_specs=[anywhere] * 5,
         out_specs=[vmem] * 4,

time: 93.8 us -> 89 us (0.949)
  local copies, waits for them, and re-layouts: 3.71 us -> 0 us
    unnamed x8 -> x0, local copies, waits for them, and re-layouts: 3.71 us -> none
    pallas_call x1, Pallas kernels: 88.3 us -> 87.4 us  [on_device(): pl.pallas_call(kernel, out_shape=(pltpu.VMEM((128, 2048), BF16), pltpu.VM...]
where the time goes in v4:
time: 89 us; the launch traced here: 88.9 us
  Pallas kernels  88.3 us (99%)
    pallas_call x1, Pallas kernels, on_device(): pl.pallas_call(kernel, out_shape=(pltpu.VMEM((128, 2048), BF16), pltpu.VM...  87.4 us

profile of v4, /device:TPU:1, one launch (start us, length us, event | category | flops | bytes accessed | tf_op | source)
XLA Modules:
  0.0 88.9 jit_solution(11091204460265496605)
XLA Ops:
  0.6 87.4 %shard_map.84 = (bf16[128,2048]{1,0:T(8,128)(2,1)S(1)}, f32[32,768]{1,0:T(8,128)S(1)}, f32[32,768]{1,0:T(8,128)S(1)}, f32[32,768]{1,0:T(8,128)S(1)}) custom-call(bf16[128,2048]{1,0:T(8,128)(2,1)} %tok_hbm.1, bf16[128,2048]{1,0:T(8,128)(2,1)} %cot_hbm.1, bf16[2048,768]{1,0:T(8,128)(2,1)} %wg_hbm.1, bf16[2048,768]{1,0:T(8,128)(2,1)} %wu_hbm.1, ...), custom_call_target="tpu_custom_call" | custom-call | tf_op jit(solution)/shard_map/pallas_call | solution.py:472
  88.0 0.9 %shard_map.85 = (bf16[128,2048]{1,0:T(8,128)(2,1)}, f32[32,768]{1,0:T(8,128)}, f32[32,768]{1,0:T(8,128)}, f32[32,768]{1,0:T(8,128)}) custom-call(bf16[128,2048]{1,0:T(8,128)(2,1)S(1)} %get-tuple-element.8.a, f32[32,768]{1,0:T(8,128)S(1)} %get-tuple-element.9.b, f32[32,768]{1,0:T(8,128)S(1)} %get-tuple-element.10.c, f32[32,768]{1,0:T(8,128)S(1)} %get-tuple-element.11.d), custom_call_target="tpu_custom_call" | custom-call | tf_op jit(solution)/shard_map/pallas_call | solution.py:511

commit v5 on v4

--- a/solution.py
+++ b/solution.py
@@ -1,5 +1,5 @@
-import functools
 import heapq
+import itertools
 
 import jax
 import jax.numpy as jnp
@@ -15,9 +15,26 @@
 
 NY, NZ = 4, 8
 X_BEGIN, X_MIDDLE, X_END = 6.0, 14.0, 26.0
-BLOCKS = ((0, 256, "z", "r"), (256, 256, "z", "r"), (512, 128, "y", "t"), (640, 128, "y", "t"), (768, 128, "y", "t"), (896, 256, "y", "t"))
-
-
+ASIDE = tuple(("part", 0.42, 0.0) for _ in range(8)) + (("begin", 0.45, 8.5), ("middle", 0.15, 18.5), ("end", 0.3, 29.5))
+BLOCKS = (
+    (
+        (0, 256, "z", "d"),
+        (256, 256, "z", "r"),
+        (768, 128, "y", "t"),
+        (512, 256, "y", "m"),
+        (896, 128, "y", "t"),
+        (1024, 128, "z", "d"),
+    ),
+    (
+        (0, 128, "z", "r"),
+        (128, 128, "y", "r"),
+        (256, 256, "y", "r"),
+        (768, 128, "y", "m"),
+        (512, 256, "y", "t"),
+        (896, 128, "z", "r"),
+        (1024, 128, "z", "r"),
+    ),
+)
 Y_RING = ((1, 0, ((2, 1), (1, 1))), (-1, 1, ((2, 1), (1, 1))), (1, 1, ((1, 1),)), (-1, 0, ((1, 1),)))
 Z_RING = (
     (1, 0, ((4, 1), (3, 1), (2, 1), (1, 1))), (-1, 1, ((4, 1), (3, 1), (2, 1), (1, 1))),
@@ -29,15 +46,24 @@
     (-1, 0, ((3, 2), (1, 1))), (-1, 1, ((3, 2), (1, 1))),
     (1, 1, ((2, 2),)), (-1, 0, ((2, 2),)),
 )
-CHAINS = {("y", "r"): Y_RING, ("z", "r"): Z_RING, ("z", "t"): Z_TWO}
+Z_MID = (
+    (1, 0, ((4, 1), (3, 2), (1, 1))), (-1, 1, ((4, 1), (3, 2), (1, 1))),
+    (1, 1, ((3, 2), (1, 1))), (-1, 0, ((3, 2), (1, 1))),
+    (1, 0, ((2, 2),)), (1, 1, ((2, 2),)), (-1, 0, ((2, 2),)), (-1, 1, ((2, 2),)),
+)
+Y_DIRECT = (
+    (1, 0, ((2, 2),)), (-1, 1, ((2, 2),)),
+    (1, 0, ((1, 1),)), (1, 1, ((1, 1),)), (-1, 0, ((1, 1),)), (-1, 1, ((1, 1),)),
+)
+CHAINS = {("y", "r"): Y_RING, ("y", "d"): Y_DIRECT, ("z", "r"): Z_RING, ("z", "t"): Z_TWO, ("z", "m"): Z_MID}
 OFFSETS = (4, 3, -3, 2, -2, 1, -1, 0)
 SLAB = {offset: r for r, offset in enumerate(OFFSETS)}
 SLAB[-4] = 0
 
 
 class Ring:
-    def __init__(self, block, phase, axis, style, first_slot):
-        self.block, self.phase, self.axis = block, phase, axis
+    def __init__(self, block, width, phase, axis, style, first_slot):
+        self.block, self.width, self.phase, self.axis = block, width, phase, axis
         self.chains = CHAINS[axis, style]
         self.slots, at = {}, 0
         for c, (_, _, hops) in enumerate(self.chains):
@@ -47,10 +73,9 @@
         self.count, self.first_slot = at, first_slot
 
     def half_shape(self):
-        width = BLOCKS[self.block][1]
         if self.phase == 2:
-            return (32, width)
-        return (NZ // 2, 64, width) if self.axis == "y" else (NY // 2, 64, width)
+            return (32, self.width)
+        return (NZ // 2, 64, self.width) if self.axis == "y" else (NY // 2, 64, self.width)
 
     def half_bytes(self):
         size = 2
@@ -68,68 +93,114 @@
         return SLAB[self.chains[c][0] * hops[0][0]]
 
 
-def all_rings():
+def rings_of(k):
     rings, slot = {}, 0
-    for b, (_, _, first, style) in enumerate(BLOCKS):
+    for b, (_, width, first, style) in enumerate(BLOCKS[k]):
         for phase, axis in ((1, first), (2, "z" if first == "y" else "y")):
-            rings[b, phase] = Ring(b, phase, axis, "r" if phase == 1 else style, slot)
+            rings[b, phase] = Ring(b, width, phase, axis, "r" if phase == 1 else style, slot)
             slot += rings[b, phase].count
     return rings, slot
 
 
-def first_sends(rings):
-    groups = [[] for _ in OFFSETS]
-    for b in range(len(BLOCKS)):
-        ring = rings[b, 1]
-        for c in range(len(ring.chains)):
-            groups[ring.ready(c)].append((b, c))
-    return groups
-
-
-def schedule(rings, rate=46.0e3, latency=3.0, hop=0.75, step=0.06, slab=0.36):
-    free, arrivals, order, left, tick = {}, [], [], {}, [0]
-
-    def send(key, c, i, now):
-        ring = rings[key]
+def schedule(rate=46.0e3, latency=(3.0, 2.6), hop=0.75, step=0.06, slab=0.37, depth=(100.0, 2.0)):
+    tick = itertools.count()
+    rings = [rings_of(k)[0] for k in (0, 1)]
+    left = [{key: len(ring.chains) for key, ring in rings[k].items()} for k in (0, 1)]
+    inbox, ready, order = [[], []], [{}, {}], [[], []]
+    queues, backlog, free, now = {}, {}, [0.0, 0.0], 0.0
+    aside = [list(ASIDE), list(ASIDE)]
+
+    def offer(k, key, c, i):
+        ring = rings[k][key]
         sign, _, hops = ring.chains[c]
-        link = (ring.axis, sign)
-        wire = ring.half_bytes() / rate
-        start = max(free.get(link, 0.0), now)
-        free[link] = start + wire * hops[i][1]
-        tick[0] += 1
-        heapq.heappush(arrivals, (start + wire + latency + hop * (hops[i][1] - 1), tick[0], key, c, i))
-
-    for key in rings:
-        left[key] = len(rings[key].chains)
-    for r, group in enumerate(first_sends(rings)):
-        for b, c in group:
-            send((b, 1), c, 0, slab * (r + 1))
-    now = 0.0
-    while arrivals:
-        at, _, key, c, i = heapq.heappop(arrivals)
-        now = max(now, at) + step
-        order.append((now, key, c, i))
-        if i + 1 < len(rings[key].chains[c][2]):
-            send(key, c, i + 1, now)
+        rank = (1, key[0], i - len(hops)) if key[1] == 1 else (0, i - len(hops), key[0], -hops[i][1])
+        heapq.heappush(ready[k].setdefault((ring.axis, sign), []), (rank, next(tick), key, c, i))
+
+    def issue(k):
+        for link, waiting in ready[k].items():
+            while waiting and backlog.get((link, k), 0.0) / rate < depth[k]:
+                _, _, key, c, i = heapq.heappop(waiting)
+                ring = rings[k][key]
+                size = ring.half_bytes() * ring.chains[c][2][i][1]
+                queues.setdefault(link, ([], []))[k].append([size, key, c, i])
+                backlog[link, k] = backlog.get((link, k), 0.0) + size
+                order[k].append((now, "send", key, c, i))
+
+    def fill(k):
+        while aside[k]:
+            name, length, first = aside[k][0]
+            coming = inbox[k][0][0] if inbox[k] else now + 1.0
+            if free[k] < first or (coming - free[k] < 0.6 * length and free[k] < first + 4.0):
+                return
+            order[k].append((free[k], "aside", name, 0, 0))
+            free[k] += length
+            aside[k].pop(0)
+
+    for k in (0, 1):
+        for r in range(len(OFFSETS)):
+            heapq.heappush(inbox[k], (slab * (r + 1), -1, "slab", r, 0, 0))
+    while True:
+        coming = [(max(inbox[k][0][0], free[k]), 0, k, None) for k in (0, 1) if inbox[k]]
+        for link, pair in queues.items():
+            busy_now = [k for k in (0, 1) if pair[k]]
+            coming += [(now + pair[k][0][0] * len(busy_now) / (2 * rate), 1, k, link) for k in busy_now]
+        if not coming:
+            for k in (0, 1):
+                order[k] += [(now, "aside", name, 0, 0) for name, _, _ in aside[k]]
+            return order
+        at, what, k, link = min(coming, key=lambda c: c[0])
+        if at > now:
+            for line, pair in queues.items():
+                busy_now = [j for j in (0, 1) if pair[j]]
+                for j in busy_now:
+                    moved = (at - now) * 2 * rate / len(busy_now)
+                    pair[j][0][0] -= moved
+                    backlog[line, j] -= moved
+            now = at
+        if what == 1:
+            over, key, c, i = queues[link][k].pop(0)
+            backlog[link, k] -= max(over, 0.0)
+            late = latency[k] + hop * (rings[k][key].chains[c][2][i][1] - 1)
+            heapq.heappush(inbox[k], (max(now + late, slab * len(OFFSETS) + 0.01), next(tick), "take", key, c, i))
+            continue
+        _, _, kind, key, c, i = heapq.heappop(inbox[k])
+        if kind == "slab":
+            order[k].append((now, "slab", key, 0, 0))
+            for b in range(len(BLOCKS[k])):
+                ring = rings[k][b, 1]
+                for c in range(len(ring.chains)):
+                    if ring.ready(c) == key:
+                        offer(k, (b, 1), c, 0)
+            free[k] = now
         else:
-            left[key] -= 1
-            if left[key] == 0 and key[1] == 1:
-                for k in range(len(rings[key[0], 2].chains)):
-                    send((key[0], 2), k, 0, now)
-    return order, now
+            free[k] = now + step
+            order[k].append((now, "take", key, c, i))
+            if i + 1 < len(rings[k][key].chains[c][2]):
+                offer(k, key, c, i + 1)
+            else:
+                left[k][key] -= 1
+                if left[k][key] == 0 and key[1] == 1:
+                    second = (key[0], 2)
+                    for c in range(len(rings[k][second].chains)):
+                        offer(k, second, c, 0)
+        issue(k)
+        if kind == "take" or key == len(OFFSETS) - 1:
+            fill(k)
 
 
 def kernel(tok_hbm, cot_hbm, wg_hbm, wu_hbm, wd_hbm,
            ig_out, gate_out, up_out, down_out,
            xb, wgu, wd, gub, hid, acc, own_ig, ig_part, ig_send0, ig_send, ig_recv0, ig_recv,
            xr1, xr2, *rest):
-    nb = len(BLOCKS)
-    blks, rest = rest[:nb], rest[nb:]
-    rings, total_slots = all_rings()
-    keys = [(b, phase) for b in range(nb) for phase in (1, 2)]
-    rbufs, rest = dict(zip(keys, rest[: 2 * nb])), rest[2 * nb :]
-    fins, rest = rest[:nb], rest[nb:]
-    finr, rest = rest[:nb], rest[nb:]
+    blks, rbufs, fins, finr = [], [], [], []
+    for k in (0, 1):
+        nb = len(BLOCKS[k])
+        keys = [(b, phase) for b in range(nb) for phase in (1, 2)]
+        blks.append(rest[:nb])
+        rbufs.append(dict(zip(keys, rest[nb : 3 * nb])))
+        fins.append(rest[3 * nb : 4 * nb])
+        finr.append(rest[4 * nb : 5 * nb])
+        rest = rest[5 * nb :]
     (load_sem, ag_send, ag_recv, rel_send, rel_recv, igx_send, igx_recv,
      xrs_send, xrs_recv, ring_send, ring_recv, fin_send, fin_recv) = rest
 
@@ -138,10 +209,9 @@
     right = (rep, lax.rem(x + 1, 4), core)
     left = (rep, lax.rem(x + 3, 4), core)
     partner = (rep, x, 1 - core)
-    far = any(ring.chains is Z_TWO for ring in rings.values())
-    y_of = {s: (z * NY + lax.rem(y + s + NY, NY), x, core) for s in (1, -1)}
-    z_of = {s: (lax.rem(z + s + NZ, NZ) * NY + y, x, core)
-            for s in ((1, -1, 2, -2) if far else (1, -1))}
+    y_of = {s: (z * NY + lax.rem(y + s + NY, NY), x, core) for s in (1, -1, 2)}
+    y_of[-2] = y_of[2]
+    z_of = {s: (lax.rem(z + s + NZ, NZ) * NY + y, x, core) for s in (1, -1, 2, -2)}
 
     def remote(src, dst, send_sem, recv_sem, to):
         return pltpu.make_async_remote_copy(src_ref=src, dst_ref=dst, send_sem=send_sem,
@@ -161,7 +231,7 @@
         copy.start()
 
     barrier = pltpu.get_barrier_semaphore()
-    others = (right, left, partner, *y_of.values(), *z_of.values())
+    others = (right, left, partner, y_of[1], y_of[-1], y_of[2], *z_of.values())
     for other in others:
         pl.semaphore_signal(barrier, inc=1, device_id=other, device_id_type=MESH)
     pl.semaphore_wait(barrier, len(others))
@@ -206,14 +276,16 @@
         gub[rows, pl.ds(384, 384)] = (hg * act).astype(BF16)
         hid[rows, :] = (act * up).astype(BF16)
 
+    def input_slice(s, n, store):
+        rows = pl.ds(pl.multiple_of(s * 128, 128), 128)
+        d = pl.ds(pl.multiple_of(n * 512, 512), 512)
+        part = lax.dot_general(gub[rows, :], wgu[d, :], (((1,), (1,)), ((), ())),
+                               preferred_element_type=F32)
+        store(d, part.astype(BF16))
+
     def input_part(s, store):
-        rows = pl.ds(pl.multiple_of(s * 128, 128), 128)
-
         def some(n, carry):
-            d = pl.ds(pl.multiple_of(n * 512, 512), 512)
-            part = lax.dot_general(gub[rows, :], wgu[d, :], (((1,), (1,)), ((), ())),
-                                   preferred_element_type=F32)
-            store(d, part.astype(BF16))
+            input_slice(s, n, store)
             return carry
 
         lax.fori_loop(0, 4, some, 0)
@@ -229,15 +301,21 @@
     def send_ig(k):
         return remote(ig_send.at[k], ig_recv.at[k], igx_send.at[k], igx_recv.at[k], partner)
 
-    def step_part(s):
-        k = s - 2
-
+    def store_step(k):
         def store(d, part):
             ig_part[k, :, d] = part[:64]
             ig_send[k, :, d] = part[64:]
-
-        input_part(s, store)
-        send_ig(k).start()
+        return store
+
+    def step_part(s):
+        input_part(s, store_step(s - 2))
+        send_ig(s - 2).start()
+
+    def late_slice(n):
+        s = 6 + n // 4
+        input_slice(s, n % 4, store_step(s - 2))
+        if n % 4 == 3:
+            send_ig(s - 2).start()
 
     forward(0)
     input_part(0, store_own)
@@ -282,18 +360,18 @@
         acc[j, :, pl.ds(768, 384)] = b
         return carry
 
-    lax.fori_loop(0, 4, first_sums, 0)
+    lax.fori_loop(0, 2, first_sums, 0)
     take(4)
-    lax.fori_loop(4, 8, first_sums, 0)
+    lax.fori_loop(2, 5, first_sums, 0)
     relay(4).wait_recv()
     forward(6)
     take(5)
-    step_part(6)
+    lax.fori_loop(5, 8, first_sums, 0)
     relay(5).wait_recv()
     forward(7)
 
-    def half_of(ring, offset, half):
-        blk = blks[ring.block]
+    def half_of(k, ring, offset, half):
+        blk = blks[k][ring.block]
         if ring.axis == "y":
             there = lax.rem(y + offset + NY, NY)
             if ring.phase == 1:
@@ -303,13 +381,12 @@
             return blk.at[SLAB[offset], pl.ds(2 * half, 2)]
         return blk.at[SLAB[offset], y, pl.ds(32 * half, 32)]
 
-    def hop(key, c, i):
-        ring = rings[key]
+    def hop(k, ring, c, i):
         sign, half, hops = ring.chains[c]
         slot = ring.slots[c, i]
         sem = ring.first_slot + slot
-        return remote(half_of(ring, sign * hops[i][0], half), rbufs[key].at[slot],
-                      ring_send.at[sem], ring_recv.at[sem],
+        return remote(half_of(k, ring, sign * hops[i][0], half),
+                      rbufs[k][ring.block, ring.phase].at[slot], ring_send.at[sem], ring_recv.at[sem],
                       (y_of if ring.axis == "y" else z_of)[sign * hops[i][1]])
 
     def add_into(dst, src):
@@ -322,18 +399,15 @@
                 return carry
             lax.fori_loop(0, shape[0], one, 0)
 
-    for r, group in enumerate(first_sends(rings)):
+    def last_sums(k, r):
         j = lax.rem(z + OFFSETS[r] + NZ, NZ)
         a, b = products(j, 6, 2)
         a = (acc[j, :, pl.ds(0, 768)] + a).astype(BF16)
         b = (acc[j, :, pl.ds(768, 384)] + b).astype(BF16)
-        for i, (col, width, _, _) in enumerate(BLOCKS):
+        for i, (col, width, _, _) in enumerate(BLOCKS[k]):
             piece = a[:, col : col + width] if col < 768 else b[:, col - 768 : col - 768 + width]
-            blks[i][r] = piece.reshape(NY, 64, width)
-        for block, c in group:
-            hop((block, 1), c, 0).start()
-
-    step_part(7)
+            blks[k][i][r] = piece.reshape(NY, 64, width)
+
 
     def xrs(stage, way):
         rows = pl.ds(32 * way, 32)
@@ -376,63 +450,75 @@
             total = total + xr2[0, piece].astype(F32) + xr2[1, (piece + 2) % 4].astype(F32)
             ig_out[rows, :] = total.astype(BF16)
 
-    order, _ = schedule(rings)
-    left_of = {key: len(rings[key].chains) for key in keys}
     scale = float(32768) ** -0.5
 
-    def fin_copy(b):
-        return remote(fins[b].at[pl.ds(pl.multiple_of((1 - core) * 32, 32), 32)], finr[b],
+    def fin_copy(k, b):
+        return remote(fins[k][b].at[pl.ds(32 * (1 - k), 32)], finr[k][b],
                       fin_send.at[b], fin_recv.at[b], partner)
 
-    def finish_block(b):
-        ring = rings[b, 2]
+    def finish_block(k, ring):
+        b = ring.block
         for half in (0, 1):
-            total = half_of(ring, 0, half)[...].astype(F32)
+            total = half_of(k, ring, 0, half)[...].astype(F32)
             for c, (_, h, _) in enumerate(ring.chains):
                 if h == half:
-                    total = total + rbufs[b, 2][ring.last(c)].astype(F32)
-            fins[b][pl.ds(32 * half, 32), :] = total * scale
-        fin_copy(b).start()
-
-    todo = [(X_BEGIN, x_begin), (X_MIDDLE, x_middle), (X_END, x_end)]
-    for at, key, c, i in order:
-        while todo and at > todo[0][0]:
-            todo.pop(0)[1]()
-        ring = rings[key]
-        sign, half, hops = ring.chains[c]
-        hop(key, c, i).wait_recv()
-        if i + 1 < len(hops):
-            add_into(half_of(ring, sign * hops[i + 1][0], half), rbufs[key].at[ring.slots[c, i]])
-            hop(key, c, i + 1).start()
-        else:
-            left_of[key] -= 1
-            if key[1] == 1:
-                add_into(half_of(ring, 0, half), rbufs[key].at[ring.slots[c, i]])
-                if left_of[key] == 0:
-                    second = (key[0], 2)
-                    for k in range(len(rings[second].chains)):
-                        hop(second, k, 0).start()
-            elif left_of[key] == 0:
-                finish_block(key[0])
-    for _, act in todo:
-        act()
-
-    def place_out(b, value, which):
-        col, width, _, _ = BLOCKS[b]
+                    total = total + rbufs[k][b, 2][ring.last(c)].astype(F32)
+            fins[k][b][pl.ds(32 * half, 32), :] = total * scale
+        fin_copy(k, b).start()
+
+    def place_out(k, b, value):
+        col, width, _, _ = BLOCKS[k][b]
         at = col
         while at < col + width:
-            take_n = min(384 - at % 384, col + width - at)
-            out = (gate_out, up_out, down_out)[at // 384]
-            out[:, pl.ds(pl.multiple_of(which * 384 + at % 384, 128), take_n)] = (
-                value[:, at - col : at - col + take_n])
-            at += take_n
-
-    mine = pl.ds(pl.multiple_of(core * 32, 32), 32)
-    for b in range(nb):
-        place_out(b, fins[b][mine, :], core)
-    for b in range(nb):
-        fin_copy(b).wait_recv()
-        place_out(b, finr[b][...], 1 - core)
+            count = min(384 - at % 384, col + width - at)
+            which, there = at // 384, k * 384 + at % 384
+            (gate_out, up_out, down_out)[which][:, pl.ds(there, count)] = (
+                value[:, at - col : at - col + count])
+            at += count
+
+    orders = schedule()
+
+    def scatter(k):
+        rings, _ = rings_of(k)
+        left_of = {key: len(ring.chains) for key, ring in rings.items()}
+        slices = iter(range(8))
+        acts = {"part": lambda: late_slice(next(slices)), "begin": x_begin, "middle": x_middle, "end": x_end}
+        for at, what, key, c, i in orders[k]:
+            if what == "slab":
+                last_sums(k, key)
+                continue
+            if what == "aside":
+                acts[key]()
+                continue
+            ring = rings[key]
+            if what == "send":
+                hop(k, ring, c, i).start()
+                continue
+            sign, half, hops = ring.chains[c]
+            hop(k, ring, c, i).wait_recv()
+            if i + 1 < len(hops):
+                add_into(half_of(k, ring, sign * hops[i + 1][0], half),
+                         rbufs[k][key].at[ring.slots[c, i]])
+            else:
+                left_of[key] -= 1
+                if key[1] == 1:
+                    add_into(half_of(k, ring, 0, half), rbufs[k][key].at[ring.slots[c, i]])
+                elif left_of[key] == 0:
+                    finish_block(k, ring)
+        for b in range(len(BLOCKS[k])):
+            place_out(k, b, fins[k][b][pl.ds(32 * k, 32), :])
+        for b in range(len(BLOCKS[1 - k])):
+            fin_copy(1 - k, b).wait_recv()
+            place_out(1 - k, b, finr[1 - k][b][...])
+
+        for ring in rings.values():
+            for c, i in ring.slots:
+                hop(k, ring, c, i).wait_send()
+        for b in range(len(BLOCKS[k])):
+            fin_copy(k, b).wait_send()
+
+    for k in (0, 1):
+        pl.when(core == k)(lambda k=k: scatter(k))
 
     for k in range(4):
         for side in (0, 1):
@@ -448,10 +534,6 @@
     for stage in range(3):
         for way in (0, 1):
             xrs(stage, way).wait_send()
-    for _, key, c, i in order:
-        hop(key, c, i).wait_send()
-    for b in range(nb):
-        fin_copy(b).wait_send()
 
 
 def write_out(a, b, c, d, out_a, out_b, out_c, out_d, sems):
@@ -464,8 +546,9 @@
 
 
 def on_device(tokens, cotangent, gate_weight, up_weight, down_weight_t):
-    rings, slots = all_rings()
-    keys = [(b, phase) for b in range(len(BLOCKS)) for phase in (1, 2)]
+    rings = [rings_of(k)[0] for k in (0, 1)]
+    slots = max(rings_of(k)[1] for k in (0, 1))
+    most = max(len(blocks) for blocks in BLOCKS)
     anywhere = pl.BlockSpec(memory_space=pl.ANY)
     vmem = pl.BlockSpec(memory_space=pltpu.VMEM)
     dma = pltpu.SemaphoreType.DMA
@@ -495,14 +578,24 @@
             pltpu.VMEM((2, 2, 32, 2048), BF16),
             pltpu.VMEM((2, 4, 32, 2048), BF16),
         ]
-        + [pltpu.VMEM((NZ, NY, 64, width), BF16) for _, width, _, _ in BLOCKS]
-        + [pltpu.VMEM((rings[key].count, *rings[key].half_shape()), BF16) for key in keys]
-        + [pltpu.VMEM((64, width), F32) for _, width, _, _ in BLOCKS]
-        + [pltpu.VMEM((32, width), F32) for _, width, _, _ in BLOCKS]
+        + [
+            ref
+            for k in (0, 1)
+            for ref in (
+                [pltpu.VMEM((NZ, NY, 64, width), BF16) for _, width, _, _ in BLOCKS[k]]
+                + [
+                    pltpu.VMEM((rings[k][b, phase].count, *rings[k][b, phase].half_shape()), BF16)
+                    for b in range(len(BLOCKS[k]))
+                    for phase in (1, 2)
+                ]
+                + [pltpu.VMEM((64, width), F32) for _, width, _, _ in BLOCKS[k]]
+                + [pltpu.VMEM((32, width), F32) for _, width, _, _ in BLOCKS[k]]
+            )
+        ]
         + [
             dma((5,)), dma((2, 6)), dma((2, 6)), dma((7,)), dma((7,)), dma((7,)), dma((7,)),
             dma((3, 2)), dma((3, 2)), dma((slots,)), dma((slots,)),
-            dma((len(BLOCKS),)), dma((len(BLOCKS),)),
+            dma((most,)), dma((most,)),
         ],
         compiler_params=pltpu.CompilerParams(
             collective_id=0, has_side_effects=True, vmem_limit_bytes=VMEM_LIMIT

time: 89 us -> 87.5 us (0.983)
  Pallas kernels: 88.3 us -> 86.7 us
    pallas_call x1, Pallas kernels: 87.4 us -> 85.7 us  [on_device(): pl.pallas_call(kernel, out_shape=(pltpu.VMEM((128, 2048), BF16), pltpu.VM...]
where the time goes in v5:
time: 87.5 us
  Pallas kernels  86.7 us (99%)
    pallas_call x1, Pallas kernels, on_device(): pl.pallas_call(kernel, out_shape=(pltpu.VMEM((128, 2048), BF16), pltpu.VM...  85.7 us

profile of v5, /device:TPU:1, one launch (start us, length us, event | category | flops | bytes accessed | tf_op | source)
XLA Modules:
  0.0 87.5 jit_solution(6780951749980207769)
XLA Ops:
  0.6 85.7 %shard_map.84 = (bf16[128,2048]{1,0:T(8,128)(2,1)S(1)}, f32[32,768]{1,0:T(8,128)S(1)}, f32[32,768]{1,0:T(8,128)S(1)}, f32[32,768]{1,0:T(8,128)S(1)}) custom-call(bf16[128,2048]{1,0:T(8,128)(2,1)} %tok_hbm.1, bf16[128,2048]{1,0:T(8,128)(2,1)} %cot_hbm.1, bf16[2048,768]{1,0:T(8,128)(2,1)} %wg_hbm.1, bf16[2048,768]{1,0:T(8,128)(2,1)} %wu_hbm.1, ...), custom_call_target="tpu_custom_call" | custom-call | tf_op jit(solution)/shard_map/pallas_call | solution.py:555
  86.4 0.9 %shard_map.85 = (bf16[128,2048]{1,0:T(8,128)(2,1)}, f32[32,768]{1,0:T(8,128)}, f32[32,768]{1,0:T(8,128)}, f32[32,768]{1,0:T(8,128)}) custom-call(bf16[128,2048]{1,0:T(8,128)(2,1)S(1)} %get-tuple-element.8.a, f32[32,768]{1,0:T(8,128)S(1)} %get-tuple-element.9.b, f32[32,768]{1,0:T(8,128)S(1)} %get-tuple-element.10.c, f32[32,768]{1,0:T(8,128)S(1)} %get-tuple-element.11.d), custom_call_target="tpu_custom_call" | custom-call | tf_op jit(solution)/shard_map/pallas_call | solution.py:604

commit v6 on v5

--- a/solution.py
+++ b/solution.py
@@ -18,21 +18,21 @@
 ASIDE = tuple(("part", 0.42, 0.0) for _ in range(8)) + (("begin", 0.45, 8.5), ("middle", 0.15, 18.5), ("end", 0.3, 29.5))
 BLOCKS = (
     (
-        (0, 256, "z", "d"),
+        (0, 128, "y", "m"),
+        (128, 128, "y", "m"),
         (256, 256, "z", "r"),
+        (512, 256, "z", "d"),
         (768, 128, "y", "t"),
-        (512, 256, "y", "m"),
         (896, 128, "y", "t"),
         (1024, 128, "z", "d"),
     ),
     (
-        (0, 128, "z", "r"),
-        (128, 128, "y", "r"),
-        (256, 256, "y", "r"),
-        (768, 128, "y", "m"),
-        (512, 256, "y", "t"),
-        (896, 128, "z", "r"),
-        (1024, 128, "z", "r"),
+        (768, 128, "z", "r"),
+        (896, 128, "y", "r"),
+        (0, 256, "y", "r"),
+        (1024, 128, "y", "t"),
+        (256, 256, "y", "t"),
+        (512, 256, "z", "r"),
     ),
 )
 Y_RING = ((1, 0, ((2, 1), (1, 1))), (-1, 1, ((2, 1), (1, 1))), (1, 1, ((1, 1),)), (-1, 0, ((1, 1),)))
@@ -102,7 +102,7 @@
     return rings, slot
 
 
-def schedule(rate=46.0e3, latency=(3.0, 2.6), hop=0.75, step=0.06, slab=0.37, depth=(100.0, 2.0)):
+def schedule(rate=46.0e3, latency=(3.0, 2.6), hop=0.75, step=0.06, slab=0.37, depth=(3.0, 2.0)):
     tick = itertools.count()
     rings = [rings_of(k)[0] for k in (0, 1)]
     left = [{key: len(ring.chains) for key, ring in rings[k].items()} for k in (0, 1)]
@@ -362,11 +362,11 @@
 
     lax.fori_loop(0, 2, first_sums, 0)
     take(4)
-    lax.fori_loop(2, 5, first_sums, 0)
+    lax.fori_loop(2, 6, first_sums, 0)
     relay(4).wait_recv()
     forward(6)
     take(5)
-    lax.fori_loop(5, 8, first_sums, 0)
+    lax.fori_loop(6, 8, first_sums, 0)
     relay(5).wait_recv()
     forward(7)
 

time: 87.5 us -> 87.6 us (level)
  no operation moved by 1% of the time
where the time goes in v6:
time: 87.6 us
  Pallas kernels  86.8 us (99%)
    pallas_call x1, Pallas kernels, on_device(): pl.pallas_call(kernel, out_shape=(pltpu.VMEM((128, 2048), BF16), pltpu.VM...  85.8 us

profile of v6, /device:TPU:1, one launch (start us, length us, event | category | flops | bytes accessed | tf_op | source)
XLA Modules:
  0.0 87.6 jit_solution(6070084300628189090)
XLA Ops:
  0.6 85.8 %shard_map.84 = (bf16[128,2048]{1,0:T(8,128)(2,1)S(1)}, f32[32,768]{1,0:T(8,128)S(1)}, f32[32,768]{1,0:T(8,128)S(1)}, f32[32,768]{1,0:T(8,128)S(1)}) custom-call(bf16[128,2048]{1,0:T(8,128)(2,1)} %tok_hbm.1, bf16[128,2048]{1,0:T(8,128)(2,1)} %cot_hbm.1, bf16[2048,768]{1,0:T(8,128)(2,1)} %wg_hbm.1, bf16[2048,768]{1,0:T(8,128)(2,1)} %wu_hbm.1, ...), custom_call_target="tpu_custom_call" | custom-call | tf_op jit(solution)/shard_map/pallas_call | solution.py:555
  86.5 0.9 %shard_map.85 = (bf16[128,2048]{1,0:T(8,128)(2,1)}, f32[32,768]{1,0:T(8,128)}, f32[32,768]{1,0:T(8,128)}, f32[32,768]{1,0:T(8,128)}) custom-call(bf16[128,2048]{1,0:T(8,128)(2,1)S(1)} %get-tuple-element.8.a, f32[32,768]{1,0:T(8,128)S(1)} %get-tuple-element.9.b, f32[32,768]{1,0:T(8,128)S(1)} %get-tuple-element.10.c, f32[32,768]{1,0:T(8,128)S(1)} %get-tuple-element.11.d), custom_call_target="tpu_custom_call" | custom-call | tf_op jit(solution)/shard_map/pallas_call | solution.py:604
